TPU v7x, 512 devices: a whole 4x4x16 slice. The times are simulated.
512 devices in a mesh: ep: 128 (over z, x, core), tp: 4 (over y).
Axes of the slice: x: 4, y: 4, z: 16, core: 2. Of those that a mesh axis runs over, the one named last changes fastest.
Arguments:
- tokens: bfloat16 [16384, 2048], P('ep', 'tp'), may hold values from -6 to 6
- cotangent: bfloat16 [16384, 2048], P('ep', 'tp'), may hold values from -6 to 6
- experts: int32 [16384, 2], P('ep'), may hold values from 0 to 127, as said below
- combine: float32 [16384, 2], P('ep'), may hold values from 0.2 to 1
- w_gate: bfloat16 [128, 2048, 256], P('ep', 'tp'), may hold values from -0.125 to 0.125
- w_up: bfloat16 [128, 2048, 256], P('ep', 'tp'), may hold values from -0.125 to 0.125
- w_down: bfloat16 [128, 256, 2048], P('ep', None, 'tp'), may hold values from -0.375 to 0.375
Outputs:
- grad_tokens: bfloat16 [16384, 2048], P('ep', 'tp')
- grad_combine: float32 [16384, 2], P('ep')
- gate_grad: float32 [128, 2048, 256], P('ep', 'tp')
- up_grad: float32 [128, 2048, 256], P('ep', 'tp')
- down_grad: float32 [128, 256, 2048], P('ep', None, 'tp')
Inputs may be any that keep to these rules, and one draw needn't show every extreme that they name: Each row names two different experts of one group of 4 consecutive experts. The rows of one index of ep name any one expert at most 4 times, and some expert exactly 4 times.
All inputs are finite; a program needn't handle non-finite values.
Results may differ from a plain program's by a relative error of at most 0.019.
Values may be sent and summed in bfloat16 or wider, within the bound.
No kernel may reach another device: no remote copies, remote signals or barrier semaphores. Data moves between devices by JAX's collectives and lax.ppermute only.
A program may use at most 64 MiB of HBM per device.

v0:
```python
import jax
import jax.numpy as jnp
from jax import lax
from jax.sharding import PartitionSpec as P


def sent_together(arrays, axis, split_dim, concat_dim, along):
    columns = [a.reshape(*a.shape[:along], -1) for a in arrays]
    both = jnp.concatenate(columns, axis=along)
    whole, at, finished = (
        lax.all_to_all(both, axis, split_axis=split_dim, concat_axis=concat_dim, tiled=True),
        0,
        [],
    )
    for a, column in zip(arrays, columns):
        piece = whole[..., at : at + column.shape[along]]
        finished.append(piece.reshape(*piece.shape[:along], *a.shape[along:]))
        at += column.shape[along]
    return tuple(finished)


def cut_along(shard, dim, devices):
    dims = shard.shape
    pieces = shard.reshape(*dims[:dim], devices, dims[dim] // devices, *dims[dim + 1 :])
    return jnp.moveaxis(pieces, dim, 0)


def summed_on_arrival(shard, axis, dim):
    pieces = cut_along(shard, dim, lax.axis_size(axis))
    arrived = lax.all_to_all(pieces, axis, split_axis=0, concat_axis=0, tiled=True)
    return arrived.astype(jnp.float32).sum(axis=0)


def side_by_side(arrays, axis, dim, along):
    ends, at = ([], 0)
    for a in arrays[:-1]:
        at += a.shape[along]
        ends.append(at)
    both = jnp.concatenate(arrays, axis=along)
    return tuple(jnp.split(summed_on_arrival(both, axis, dim), ends, axis=along))


def side_by_side_2(arrays, axis, dim, along):
    ends, at = ([], 0)
    for a in arrays[:-1]:
        at += a.shape[along]
        ends.append(at)
    both = jnp.concatenate(arrays, axis=along)
    return tuple(jnp.split(lax.all_gather(both, axis, axis=dim, tiled=True), ends, axis=along))


def sent_to_all(shard, axis):
    copies = jnp.broadcast_to(shard, (lax.axis_size(axis), *shard.shape))
    return lax.all_to_all(copies, axis, split_axis=0, concat_axis=0, tiled=True)


def joined_along(pieces, dim):
    pieces = jnp.moveaxis(pieces, 0, dim)
    dims = pieces.shape
    return pieces.reshape(*dims[:dim], dims[dim] * dims[dim + 1], *dims[dim + 2 :])


def gathered_copies(shard, axis, dim):
    pieces = sent_to_all(shard, axis)
    return joined_along(pieces, dim)


def slot_positions(routed, total_experts, capacity):
    onehot = (routed[:, None] == jnp.arange(total_experts, dtype=jnp.int32)[None, :]).astype(
        jnp.int32
    )
    earlier = jnp.sum((jnp.cumsum(onehot, axis=0) - onehot) * onehot, axis=1)
    return routed * capacity + earlier


def activation(gate_pre, up_pre, grad_scaled, weight_grid):
    sigmoid_val = jax.nn.sigmoid(gate_pre)
    silu_val = gate_pre * sigmoid_val
    hidden = silu_val * up_pre
    scaled = (weight_grid * hidden).astype(jnp.bfloat16)
    comb_part = jnp.sum(hidden * grad_scaled, axis=3)
    grad_hidden = weight_grid * grad_scaled
    grad_gate_pre = (
        grad_hidden * up_pre * sigmoid_val * (1.0 + gate_pre * (1.0 - sigmoid_val))
    ).astype(jnp.bfloat16)
    grad_up_pre = (grad_hidden * silu_val).astype(jnp.bfloat16)
    return (scaled, grad_gate_pre, grad_up_pre, comb_part)


def body(tokens, cotangent, experts, combine, w_gate, w_up, w_down):
    peers = lax.axis_size("ep")
    widths = lax.axis_size("tp")
    local_experts = w_gate.shape[0]
    total_experts = local_experts * peers
    tok_count = tokens.shape[0]
    picks = experts.shape[1]
    assigns = tok_count * picks
    capacity = 2 * assigns // total_experts
    per_peer = local_experts * capacity
    block_width = tokens.shape[1]
    slot_index = slot_positions(experts.reshape(assigns), total_experts, capacity)
    slot_owner = (
        jnp.zeros((total_experts * capacity,), jnp.int32)
        .at[slot_index]
        .set(jnp.arange(assigns, dtype=jnp.int32) + 1)
    )
    filled = slot_owner > 0
    source = jnp.maximum(slot_owner - 1, 0)
    token_ids = source // picks
    filled_col = filled[:, None]
    send_rows = jnp.where(
        filled_col, jnp.take(tokens, token_ids, axis=0), jnp.zeros((), jnp.bfloat16)
    ).reshape(peers, per_peer, block_width)
    send_cots = jnp.where(
        filled_col, jnp.take(cotangent, token_ids, axis=0), jnp.zeros((), jnp.bfloat16)
    ).reshape(peers, per_peer, block_width)
    send_weights = (
        jnp.where(filled, jnp.take(combine.reshape(assigns), source), jnp.float32(0.0))
        .astype(jnp.bfloat16)
        .reshape(peers, per_peer)
    )
    recv_rows, recv_cots, recv_weights = sent_together(
        (send_rows, send_cots, send_weights), "ep", 0, 0, 2
    )
    rows_grid = recv_rows.reshape(peers, local_experts, capacity, block_width)
    cots_grid = recv_cots.reshape(peers, local_experts, capacity, block_width)
    weight_grid = recv_weights.astype(jnp.float32).reshape(peers, local_experts, capacity, 1)
    gate_part = jnp.einsum(
        "secd,edf->secf", rows_grid, w_gate, preferred_element_type=jnp.float32
    ).astype(jnp.bfloat16)
    up_part = jnp.einsum(
        "secd,edf->secf", rows_grid, w_up, preferred_element_type=jnp.float32
    ).astype(jnp.bfloat16)
    down_part = jnp.einsum(
        "secd,efd->secf", cots_grid, w_down, preferred_element_type=jnp.float32
    ).astype(jnp.bfloat16)
    share_peers = peers // widths
    gate_pre, up_pre, grad_scaled = side_by_side((gate_part, up_part, down_part), "tp", 0, 1)
    weight_share = lax.dynamic_slice_in_dim(
        weight_grid, lax.axis_index("tp") * share_peers, share_peers, 0
    )
    scaled_share, gate_share, up_share, comb_share = activation(
        gate_pre, up_pre, grad_scaled, weight_share
    )
    scaled, grad_gate_pre, grad_up_pre = side_by_side_2(
        (scaled_share, gate_share, up_share), "tp", 0, 1
    )
    comb_part = gathered_copies(comb_share, "tp", 0)
    down_grad = jnp.einsum("secf,secd->efd", scaled, cots_grid, preferred_element_type=jnp.float32)
    gate_grad = jnp.einsum(
        "secd,secf->edf", rows_grid, grad_gate_pre, preferred_element_type=jnp.float32
    )
    up_grad = jnp.einsum(
        "secd,secf->edf", rows_grid, grad_up_pre, preferred_element_type=jnp.float32
    )
    slot_sum = jnp.einsum(
        "secf,edf->secd", grad_gate_pre, w_gate, preferred_element_type=jnp.float32
    )
    slot_sum = slot_sum + jnp.einsum(
        "secf,edf->secd", grad_up_pre, w_up, preferred_element_type=jnp.float32
    )
    slot_grad = slot_sum.astype(jnp.bfloat16).reshape(peers, per_peer, block_width)
    returned = lax.all_to_all(slot_grad, "ep", split_axis=0, concat_axis=0, tiled=True)
    comb_back = lax.all_to_all(
        comb_part.reshape(peers, per_peer), "ep", split_axis=0, concat_axis=0, tiled=True
    )
    full_grad = returned.reshape(total_experts * capacity, block_width)
    per_assign = (
        jnp.take(full_grad, slot_index, axis=0)
        .astype(jnp.float32)
        .reshape(tok_count, picks, block_width)
    )
    grad_tokens = jnp.sum(per_assign, axis=1).astype(jnp.bfloat16)
    grad_combine = jnp.take(comb_back.reshape(total_experts * capacity), slot_index).reshape(
        tok_count, picks
    )
    return (grad_tokens, grad_combine, gate_grad, up_grad, down_grad)


def solution(mesh):
    return jax.shard_map(
        body,
        mesh=mesh,
        in_specs=(
            P("ep", "tp"),
            P("ep", "tp"),
            P("ep", None),
            P("ep", None),
            P("ep", "tp", None),
            P("ep", "tp", None),
            P("ep", None, "tp"),
        ),
        out_specs=(
            P("ep", "tp"),
            P("ep", None),
            P("ep", "tp", None),
            P("ep", "tp", None),
            P("ep", None, "tp"),
        ),
        check_vma=False,
    )
```

profile of v0, /device:TPU:6, one launch (start us, length us, event | category | flops | bytes accessed | tf_op | source)
XLA Modules:
  0.0 201.4 jit_solution(5399666280655892742)
XLA Ops:
  0.7 0.8 copy.46
  2.6 1.4 scatter_custom_fusion
  4.3 3.4 %gather_fusion = bf16[512]{0:T(512)(128)(2,1)S(1)} fusion(bf16[256]{0:T(256)(128)(2,1)S(1)} %reshape.173, s32[1024]{0:T(1024)S(1)} %pad_clamp_fusion.1), kind=kCustom, calls=%fused_computation.2 | custom fusion | bytes 4096 | tf_op jit(solution)/shard_map/jit(_take)/gather | solution.py:118
  8.0 2.0 gather_fusion.3
  10.0 2.0 gather_fusion.4
  12.4 0.6 pad_maximum_fusion
  13.0 78.9 %all_to_all.29 = bf16[128,4,1025]{2,1,0:T(4,128)(2,1)S(1)} all-to-all(bf16[128,4,1025]{2,1,0:T(4,128)(2,1)S(1)} %pad_maximum_fusion), channel_id=1, replica_groups=mesh['ep'=128,'tp'=4] {'ep'}, dimensions={0} | all-to-all | bytes 2099200 | tf_op jit(solution)/shard_map/all_to_all | solution.py:11
  92.3 0.6 copy-done.3
  93.9 0.9 copy.56
  94.9 4.5 %all-to-all-start.1 = ((bf16[4,32,3,4,256]{4,1,3,2,0:T(8,128)(2,1)}), bf16[4,32,3,4,256]{4,1,3,2,0:T(8,128)(2,1)S(1)}, u32[]{:S(2)}, u32[]{:S(2)}) async-start(bf16[4,32,3,4,256]{4,1,3,2,0:T(8,128)(2,1)} %copy.56), calls=%async_computation.1 | async-start | bytes 1572864 | tf_op jit(solution)/shard_map/all_to_all | solution.py:30
  99.5 12.7 %all-to-all-done.1 = bf16[4,32,3,4,256]{4,1,3,2,0:T(8,128)(2,1)S(1)} async-done(((bf16[4,32,3,4,256]{4,1,3,2,0:T(8,128)(2,1)}), bf16[4,32,3,4,256]{4,1,3,2,0:T(8,128)(2,1)S(1)}, u32[]{:S(2)}, u32[]{:S(2)}) %all-to-all-start.1) | async-done | bytes 786464 | tf_op jit(solution)/shard_map/all_to_all | solution.py:30
  112.6 14.3 %all_gather.3 = bf16[128,3,4,256]{3,0,2,1:T(8,128)(2,1)S(1)} all-gather(bf16[32,3,4,256]{3,0,2,1:T(8,128)(2,1)S(1)} %pad_maximum_fusion.2), channel_id=1, replica_groups=mesh['ep'=128,'tp'=4] {'tp'}, dimensions={0}, use_global_device_ids=true | all-gather | bytes 983040 | tf_op jit(solution)/shard_map/all_gather | solution.py:49
  126.8 0.7 reshape.255
  127.5 3.2 %all-to-all-start.3 = ((f32[4,1,128]{2,1,0:T(1,128)}), f32[4,1,128]{2,1,0:T(1,128)S(1)}, u32[]{:S(2)}, u32[]{:S(2)}) async-start(f32[4,1,128]{2,1,0:T(1,128)} %reshape.255), calls=%async_computation.3 | async-start | bytes 4096 | tf_op jit(solution)/shard_map/all_to_all | solution.py:54
  131.1 4.8 %all-to-all-done.3 = f32[4,1,128]{2,1,0:T(1,128)S(1)} async-done(((f32[4,1,128]{2,1,0:T(1,128)}), f32[4,1,128]{2,1,0:T(1,128)S(1)}, u32[]{:S(2)}, u32[]{:S(2)}) %all-to-all-start.3) | async-done | bytes 2080 | tf_op jit(solution)/shard_map/all_to_all | solution.py:54
  135.9 0.5 broadcast.146
  136.4 0.7 reduce.6
  137.2 0.7 copy.67
  137.9 7.2 %all-to-all-start.4 = ((f32[128,1,4]{2,1,0:T(1,128)}), f32[128,1,4]{2,1,0:T(1,128)S(1)}, u32[]{:S(2)}, u32[]{:S(2)}) async-start(f32[128,1,4]{2,1,0:T(1,128)} %bitcast.24), calls=%async_computation.4 | async-start | bytes 131072 | tf_op jit(solution)/shard_map/all_to_all | solution.py:164
  145.1 1.3 fusion
  146.4 1.2 copy.57
  147.6 11.2 %all-to-all-done.4 = f32[128,1,4]{2,1,0:T(1,128)S(1)} async-done(((f32[128,1,4]{2,1,0:T(1,128)}), f32[128,1,4]{2,1,0:T(1,128)S(1)}, u32[]{:S(2)}, u32[]{:S(2)}) %all-to-all-start.4) | async-done | bytes 2080 | tf_op jit(solution)/shard_map/all_to_all | solution.py:164
  158.8 6.9 %all-to-all-start.2 = ((bf16[128,4,512]{2,1,0:T(4,128)(2,1)}), bf16[128,4,512]{2,1,0:T(4,128)(2,1)S(1)}, u32[]{:S(2)}, u32[]{:S(2)}) async-start(bf16[128,4,512]{2,1,0:T(4,128)(2,1)} %copy.57), calls=%async_computation.2 | async-start | bytes 1048576 | tf_op jit(solution)/shard_map/all_to_all | solution.py:163
  165.8 1.1 convolution_bitcast_fusion.2
  167.0 1.1 convolution_bitcast_fusion.1
  168.1 1.1 convolution_bitcast_fusion
  169.7 0.8 reduce.5
  170.7 1.9 gather_fusion.2
  172.8 0.6 copy.63
  173.4 25.3 %all-to-all-done.2 = bf16[128,4,512]{2,1,0:T(4,128)(2,1)S(1)} async-done(((bf16[128,4,512]{2,1,0:T(4,128)(2,1)}), bf16[128,4,512]{2,1,0:T(4,128)(2,1)S(1)}, u32[]{:S(2)}, u32[]{:S(2)}) %all-to-all-start.2) | async-done | bytes 524320 | tf_op jit(solution)/shard_map/all_to_all | solution.py:163
  198.9 1.2 gather_fusion.1
  200.1 1.3 fusion.10
  (59 shorter events, 5.6 us)
Async XLA Ops:
  0.6 92.5 %copy-start = (bf16[1,512,256]{2,1,0:T(8,128)(2,1)S(1)}, bf16[1,512,256]{2,1,0:T(8,128)(2,1)}, u32[]{:S(2)}) copy-start(bf16[1,512,256]{2,1,0:T(8,128)(2,1)} %param.13) | copy-start | bytes 786436
  0.6 3.3 %copy-start.4 = (f32[128,2]{0,1:T(2,128)S(1)}, f32[128,2]{0,1:T(2,128)}, u32[]{:S(2)}) copy-start(f32[128,2]{0,1:T(2,128)} %param.12) | copy-start | bytes 3076
  1.6 6.3 %copy-start.1 = (bf16[128,512]{1,0:T(8,128)(2,1)S(1)}, bf16[128,512]{1,0:T(8,128)(2,1)}, u32[]{:S(2)}) copy-start(bf16[128,512]{1,0:T(8,128)(2,1)} %param.9) | copy-start | bytes 393220
  8.0 2.0 copy-start.2
  91.9 1.0 copy-start.3
  92.2 1.2 copy-start.5
  94.9 17.3 %all-to-all-start.1 = ((bf16[4,32,3,4,256]{4,1,3,2,0:T(8,128)(2,1)}), bf16[4,32,3,4,256]{4,1,3,2,0:T(8,128)(2,1)S(1)}, u32[]{:S(2)}, u32[]{:S(2)}) async-start(bf16[4,32,3,4,256]{4,1,3,2,0:T(8,128)(2,1)} %copy.56), calls=%async_computation.1 | async-start | bytes 1572864 | tf_op jit(solution)/shard_map/all_to_all | solution.py:30
  127.5 8.4 %all-to-all-start.3 = ((f32[4,1,128]{2,1,0:T(1,128)}), f32[4,1,128]{2,1,0:T(1,128)S(1)}, u32[]{:S(2)}, u32[]{:S(2)}) async-start(f32[4,1,128]{2,1,0:T(1,128)} %reshape.255), calls=%async_computation.3 | async-start | bytes 4096 | tf_op jit(solution)/shard_map/all_to_all | solution.py:54
  137.9 20.9 %all-to-all-start.4 = ((f32[128,1,4]{2,1,0:T(1,128)}), f32[128,1,4]{2,1,0:T(1,128)S(1)}, u32[]{:S(2)}, u32[]{:S(2)}) async-start(f32[128,1,4]{2,1,0:T(1,128)} %bitcast.24), calls=%async_computation.4 | async-start | bytes 131072 | tf_op jit(solution)/shard_map/all_to_all | solution.py:164
  158.8 39.9 %all-to-all-start.2 = ((bf16[128,4,512]{2,1,0:T(4,128)(2,1)}), bf16[128,4,512]{2,1,0:T(4,128)(2,1)S(1)}, u32[]{:S(2)}, u32[]{:S(2)}) async-start(bf16[128,4,512]{2,1,0:T(4,128)(2,1)} %copy.57), calls=%async_computation.2 | async-start | bytes 1048576 | tf_op jit(solution)/shard_map/all_to_all | solution.py:163
where the time goes:
time: 202 us; the launch traced here: 201 us
  blocking collectives  93.2 us (46%)
  waiting for transfers between devices  54 us (27%)
  starting transfers between devices  21.8 us (11%)
  local copies, waits for them, and re-layouts  21 us (10%)
  matrix products  5.99 us (3%)
  other arithmetic  4.5 us (2%)
    all_to_all x1, blocking collectives, sent_together(): lax.all_to_all(both, axis, split_axis=split_dim, concat_axis=concat_dim,...  78.9 us
    all_to_all x1, waiting for transfers between devices, body(): lax.all_to_all(slot_grad, 'ep', split_axis=0, concat_axis=0, tiled=True)  25.3 us
    all_gather x1, blocking collectives, side_by_side_2(): lax.all_gather(both, axis, axis=dim, tiled=True)  14.3 us
    all_to_all x1, waiting for transfers between devices, summed_on_arrival(): lax.all_to_all(pieces, axis, split_axis=0, concat_axis=0, tiled=True)  12.7 us
    all_to_all x1, waiting for transfers between devices, body(): lax.all_to_all(comb_part.reshape(peers, per_peer), 'ep', split_axis=0, co...  11.2 us
    all_to_all x1, starting transfers between devices, body(): lax.all_to_all(comb_part.reshape(peers, per_peer), 'ep', split_axis=0, co...  7.17 us
    all_to_all x1, starting transfers between devices, body(): lax.all_to_all(slot_grad, 'ep', split_axis=0, concat_axis=0, tiled=True)  6.89 us
    all_to_all x1, waiting for transfers between devices, sent_to_all(): return lax.all_to_all(copies, axis, split_axis=0, concat_axis=0, tiled=True)  4.84 us
  transfers between devices with their start and end apart: 4, of which 4 were waited for; matrix products, arithmetic and copies ran while one was open for 5% of the time, Pallas kernels for 0%

commit v1 on v0

v1 whole, which is shorter than its diff:
```python
import jax
import jax.numpy as jnp
from jax import lax
from jax.sharding import PartitionSpec as P

BF = jnp.bfloat16
F32 = jnp.float32
GROUP = 4
CAP = 8
LANES = 128


def exchange_groups(peers):
    planes = peers // 8
    groups = []
    for low in (0, 1):
        for core in (0, 1):
            groups.append([z * 8 + x * 2 + core for z in range(planes) for x in (low, 3 - low)])
    return groups


def partner(peers, bit):
    return [(i, i ^ bit) for i in range(peers)]


def dot(a, b, contract):
    return lax.dot_general(a, b, (contract, ((), ())), preferred_element_type=F32)


def split_hi_lo(v):
    hi = v.astype(BF)
    return hi, (v - hi.astype(F32)).astype(BF)


def body(tokens, cotangent, experts, combine, w_gate, w_up, w_down):
    peers = lax.axis_size("ep")
    widths = lax.axis_size("tp")
    tok_count, block = tokens.shape
    hidden = w_gate.shape[2]
    n_groups = peers // GROUP
    slots = n_groups * CAP
    share = slots // widths
    groups = exchange_groups(peers)
    mine = lax.axis_index("ep") % GROUP

    gu = jnp.concatenate([w_gate[0], w_up[0]], axis=0)
    gu_x = lax.ppermute(gu, "ep", partner(peers, 2))
    wd_x = lax.ppermute(w_down[0], "ep", partner(peers, 2))
    gu2 = jnp.stack([gu, gu_x])
    wd2 = jnp.stack([w_down[0], wd_x])
    gu4 = jnp.concatenate([gu2, lax.ppermute(gu2, "ep", partner(peers, 1))])
    wd4 = jnp.concatenate([wd2, lax.ppermute(wd2, "ep", partner(peers, 1))])
    order = (0, 2, 1, 3)
    wg4, wu4 = gu4[:, :block], gu4[:, block:]

    group = experts[:, 0] // GROUP
    same = (group[:, None] == group[None, :]) & (
        jnp.arange(tok_count)[None, :] < jnp.arange(tok_count)[:, None]
    )
    slot = group * CAP + jnp.sum(same.astype(jnp.int32), axis=1)
    place = (jnp.arange(slots)[:, None] == slot[None, :]).astype(BF)
    local = experts % GROUP
    weight_b = combine.astype(BF)
    lane = jnp.arange(LANES)[None, :]
    meta = jnp.where(lane == local[:, :1], weight_b[:, :1], 0) + jnp.where(
        lane == local[:, 1:], weight_b[:, 1:], 0
    )
    rows_out = jnp.concatenate([tokens, cotangent, meta.astype(BF)], axis=1)
    payload = dot(place, rows_out, ((1,), (0,))).astype(BF).reshape(n_groups, CAP, -1)
    arrived = lax.all_to_all(
        payload, "ep", split_axis=0, concat_axis=0, tiled=True, axis_index_groups=groups
    ).reshape(slots, -1)
    rows = arrived[:, :block]
    cots = arrived[:, block : 2 * block]
    w4 = arrived[:, 2 * block : 2 * block + GROUP].astype(F32)
    used = w4 > 0
    before = jnp.cumsum(used.astype(jnp.int32), axis=1) - used
    picks_abs = [used & (before == k) for k in (0, 1)]
    picks = [
        [jnp.any(p & (jnp.arange(GROUP)[None, :] == (mine ^ r)), axis=1, keepdims=True) for r in order]
        for p in picks_abs
    ]

    def picked(dense):
        out = []
        for k in (0, 1):
            acc = jnp.zeros(dense[0].shape, F32)
            for r in range(GROUP):
                acc = jnp.where(picks[k][r], dense[r], acc)
            out.append(acc.astype(BF))
        return out

    gate = picked([dot(rows, wg4[r], ((1,), (0,))) for r in range(GROUP)])
    up = picked([dot(rows, wu4[r], ((1,), (0,))) for r in range(GROUP)])
    down = picked([dot(cots, wd4[r], ((1,), (1,))) for r in range(GROUP)])
    parts = jnp.concatenate(
        [gate[0], up[0], down[0], gate[1], up[1], down[1]], axis=1
    ).reshape(widths, share, 6 * hidden)
    sums = (
        lax.all_to_all(parts, "tp", split_axis=0, concat_axis=0, tiled=True)
        .astype(F32)
        .sum(axis=0)
    )
    w_pick = [jnp.sum(jnp.where(p, w4, 0.0), axis=1, keepdims=True) for p in picks_abs]
    me = lax.axis_index("tp")
    sent, combs = [], []
    for k in (0, 1):
        w = lax.dynamic_slice_in_dim(w_pick[k], me * share, share, 0)
        gate_pre, up_pre, grad_scaled = (
            sums[:, (3 * k + i) * hidden : (3 * k + i + 1) * hidden] for i in range(3)
        )
        sig = jax.nn.sigmoid(gate_pre)
        silu = gate_pre * sig
        hid = silu * up_pre
        gh = w * grad_scaled
        sent.append((w * hid).astype(BF))
        sent.append((gh * up_pre * sig * (1.0 + gate_pre * (1.0 - sig))).astype(BF))
        sent.append((gh * silu).astype(BF))
        combs.extend(split_hi_lo(jnp.sum(hid * grad_scaled, axis=1, keepdims=True)))
    pad = jnp.zeros((share, LANES - 4), BF)
    acts = lax.all_gather(
        jnp.concatenate(sent + combs + [pad], axis=1), "tp", axis=0, tiled=True
    )

    def spread(i):
        a = [acts[:, (3 * k + i) * hidden : (3 * k + i + 1) * hidden] for k in (0, 1)]
        zero = jnp.zeros((), BF)
        return [
            jnp.where(picks[0][r], a[0], jnp.where(picks[1][r], a[1], zero)) for r in range(GROUP)
        ]

    scaled4, ggp4, gup4 = spread(0), spread(1), spread(2)
    slot_sum = sum(
        dot(ggp4[r], wg4[r], ((1,), (1,))) + dot(gup4[r], wu4[r], ((1,), (1,)))
        for r in range(GROUP)
    )
    back = jnp.concatenate(
        [slot_sum.astype(BF), acts[:, 6 * hidden : 6 * hidden + LANES]], axis=1
    ).reshape(n_groups, CAP, -1)
    returned = lax.all_to_all(
        back, "ep", split_axis=0, concat_axis=0, tiled=True, axis_index_groups=groups
    ).reshape(slots, -1)

    def partials(r):
        return (
            dot(rows, ggp4[r], ((0,), (0,))),
            dot(rows, gup4[r], ((0,), (0,))),
            dot(scaled4[r], cots, ((0,), (0,))),
        )

    part = [partials(r) for r in range(GROUP)]
    sib_gu = jnp.stack([jnp.concatenate(part[r][:2]).astype(BF) for r in (2, 3)])
    sib_d = jnp.stack([part[r][2].astype(BF) for r in (2, 3)])
    got_gu = lax.ppermute(sib_gu, "ep", partner(peers, 1)).astype(F32)
    got_d = lax.ppermute(sib_d, "ep", partner(peers, 1)).astype(F32)
    half_gu = [jnp.concatenate(part[r][:2]) + got_gu[r] for r in (0, 1)]
    half_d = [part[r][2] + got_d[r] for r in (0, 1)]
    total_gu = half_gu[0] + lax.ppermute(half_gu[1].astype(BF), "ep", partner(peers, 2)).astype(F32)
    total_d = half_d[0] + lax.ppermute(half_d[1].astype(BF), "ep", partner(peers, 2)).astype(F32)

    found = dot(place, returned, ((0,), (0,)))
    grad_tokens = found[:, :block].astype(BF)
    comb = [found[:, block + 2 * k : block + 2 * k + 1] + found[:, block + 2 * k + 1 : block + 2 * k + 2] for k in (0, 1)]
    first = local[:, :1] < local[:, 1:]
    grad_combine = jnp.concatenate(
        [jnp.where(first, comb[0], comb[1]), jnp.where(first, comb[1], comb[0])], axis=1
    )
    return (grad_tokens, grad_combine, total_gu[None, :block], total_gu[None, block:], total_d[None])


def solution(mesh):
    return jax.shard_map(
        body,
        mesh=mesh,
        in_specs=(
            P("ep", "tp"),
            P("ep", "tp"),
            P("ep", None),
            P("ep", None),
            P("ep", "tp", None),
            P("ep", "tp", None),
            P("ep", None, "tp"),
        ),
        out_specs=(
            P("ep", "tp"),
            P("ep", None),
            P("ep", "tp", None),
            P("ep", "tp", None),
            P("ep", None, "tp"),
        ),
        check_vma=False,
    )
```

time: 202 us -> 168 us (0.83)
  blocking collectives: 93.2 us -> 13.6 us
  starting transfers between devices: 21.8 us -> 50.9 us
  matrix products: 5.99 us -> 26.8 us
  local copies, waits for them, and re-layouts: 21 us -> 5.56 us
  other arithmetic: 4.5 us -> 17.7 us
  waiting for transfers between devices: 54 us -> 51.1 us
    all_to_all x1 -> x0, blocking collectives: 78.9 us -> none  [sent_together(): lax.all_to_all(both, axis, split_axis=split_dim, concat_axis=concat_dim,...]
    all_to_all x4 -> x3, waiting for transfers between devices: 54 us -> 26.8 us  [the longest x1 10.4 us: body(): lax.all_to_all(parts, 'tp', split_axis=0, concat_axis=0, tiled=True)]
    ppermute x0 -> x8, waiting for transfers between devices: none -> 24.3 us  [the longest x1 14.7 us: body(): wd_x = lax.ppermute(w_down[0], 'ep', partner(peers, 2))]
    dot_general x8 -> x34, matrix products: 5.99 us -> 26.8 us  [dot(): lax.dot_general(a, b, (contract, ((), ())), preferred_element_type=F32)]
    ppermute x0 -> x8, starting transfers between devices: none -> 18.6 us  [the longest x1 3.92 us: body(): wd_x = lax.ppermute(w_down[0], 'ep', partner(peers, 2))]
    gather x7 -> x0, local copies, waits for them, and re-layouts: 10.6 us -> none  [the longest x1 3.36 us: body(): jnp.take(combine.reshape(assigns), source)]
    all_to_all x4 -> x3, starting transfers between devices: 21.8 us -> 32.3 us  [the longest x1 17.9 us: body(): lax.all_to_all(payload, 'ep', split_axis=0, concat_axis=0, tiled=True, ax...]
    another operation x3 -> x6, other arithmetic: 0.26 us -> 5.42 us  [the longest x1 2.29 us: body(): jnp.stack([jnp.concatenate(part[r][:2]).astype(BF) for r in (2, 3)])]
  transfers between devices with their start and end apart: 4 -> 11, of which waited for: 4 -> 6; matrix products, arithmetic and copies ran while one was open for 5% -> 13% of each run, Pallas kernels for 0% -> 0%
where the time goes in v1:
time: 168 us; the launch traced here: 167 us
  waiting for transfers between devices  51.1 us (30%)
  starting transfers between devices  50.9 us (30%)
  matrix products  26.8 us (16%)
  other arithmetic  17.7 us (11%)
  blocking collectives  13.6 us (8%)
  local copies, waits for them, and re-layouts  5.56 us (3%)
    dot_general x34, matrix products, dot(): lax.dot_general(a, b, (contract, ((), ())), preferred_element_type=F32)  26.8 us
    all_to_all x1, starting transfers between devices, body(): lax.all_to_all(payload, 'ep', split_axis=0, concat_axis=0, tiled=True, ax...  17.9 us
    ppermute x1, waiting for transfers between devices, body(): wd_x = lax.ppermute(w_down[0], 'ep', partner(peers, 2))  14.7 us
    all_gather x1, blocking collectives, body(): lax.all_gather(jnp.concatenate(sent + combs + [pad], axis=1), 'tp', axis=...  13.6 us
    all_to_all x1, waiting for transfers between devices, body(): lax.all_to_all(parts, 'tp', split_axis=0, concat_axis=0, tiled=True)  10.4 us
    all_to_all x1, starting transfers between devices, body(): lax.all_to_all(back, 'ep', split_axis=0, concat_axis=0, tiled=True, axis_...  9.93 us
    all_to_all x1, waiting for transfers between devices, body(): lax.all_to_all(payload, 'ep', split_axis=0, concat_axis=0, tiled=True, ax...  8.39 us
    all_to_all x1, waiting for transfers between devices, body(): lax.all_to_all(back, 'ep', split_axis=0, concat_axis=0, tiled=True, axis_...  8.08 us
  transfers between devices with their start and end apart: 11, of which 6 were waited for; matrix products, arithmetic and copies ran while one was open for 13% of the time, Pallas kernels for 0%

profile of v1, /device:TPU:6, one launch (start us, length us, event | category | flops | bytes accessed | tf_op | source)
XLA Modules:
  0.0 166.9 jit_solution(10466426438612868676)
XLA Ops:
  5.6 2.1 %fusion = bf16[32,8,1152]{2,1,0:T(8,128)(2,1)} fusion(bf16[128,128]{1,0:T(8,128)(2,1)S(1)} %fusion.95, bf16[128,512]{1,0:T(8,128)(2,1)} %param.8, bf16[128,512]{1,0:T(8,128)(2,1)} %param.7, s32[128]{0:T(128)S(1)} %multiply_add_fusion), kind=kOutput, calls=%fused_computation.1 | convolution fusion | flops 76709888 | bytes 885248 | tf_op jit(solution)/shard_map/dot_general | solution.py:27
  7.7 17.9 %all-to-all-start = ((bf16[32,8,1152]{2,1,0:T(8,128)(2,1)}), bf16[32,8,1152]{2,1,0:T(8,128)(2,1)S(1)}, u32[]{:S(2)}, u32[]{:S(2)}) async-start(bf16[32,8,1152]{2,1,0:T(8,128)(2,1)} %fusion), calls=%async_computation | async-start | bytes 1179648 | tf_op jit(solution)/shard_map/all_to_all | solution.py:70
  25.8 1.9 %collective-permute-start = (bf16[1024,256]{1,0:T(8,128)(2,1)S(1)}, bf16[1024,256]{1,0:T(8,128)(2,1)S(1)}, u32[]{:S(2)}, u32[]{:S(2)}) collective-permute-start(bf16[1024,256]{1,0:T(8,128)(2,1)S(1)} %get-tuple-element.46), channel_id=1, source_target_pairs={{0,8},{4,12},{8,0},{12,4},{16,24},{20,28},{24,16},{28,20},{32,40},... | collective-permute-start | bytes 1572872 | tf_op jit(solution)/shard_map/ppermute | solution.py:47
  27.7 3.9 %collective-permute-start.2 = (bf16[256,512]{1,0:T(8,128)(2,1)S(1)}, bf16[256,512]{1,0:T(8,128)(2,1)S(1)}, u32[]{:S(2)}, u32[]{:S(2)}) collective-permute-start(bf16[256,512]{1,0:T(8,128)(2,1)S(1)} %bitcast.169), channel_id=1, source_target_pairs={{0,8},{4,12},{8,0},{12,4},{16,24},{20,28},{24,16},{28,20},{32,40},... | collective-permute-start | bytes 786440 | tf_op jit(solution)/shard_map/ppermute | solution.py:48
  31.7 14.7 %collective-permute-done.2 = bf16[256,512]{1,0:T(8,128)(2,1)S(1)} collective-permute-done((bf16[256,512]{1,0:T(8,128)(2,1)S(1)}, bf16[256,512]{1,0:T(8,128)(2,1)S(1)}, u32[]{:S(2)}, u32[]{:S(2)}) %collective-permute-start.2) | collective-permute-done | bytes 262176 | tf_op jit(solution)/shard_map/ppermute | solution.py:48
  47.2 1.9 %collective-permute-start.3 = (bf16[2,256,512]{2,1,0:T(8,128)(2,1)}, bf16[2,256,512]{2,1,0:T(8,128)(2,1)}, u32[]{:S(2)}, u32[]{:S(2)}) collective-permute-start(bf16[2,256,512]{2,1,0:T(8,128)(2,1)} %pad_maximum_fusion.2), channel_id=1, source_target_pairs={{0,4},{4,0},{8,12},{12,8},{16,20},{20,16},{24,28},{28,24},{32,36},... | collective-permute-start | bytes 1572872 | tf_op jit(solution)/shard_map/ppermute | solution.py:52
  50.4 2.4 %collective-permute-start.1 = (bf16[2,1024,256]{2,1,0:T(8,128)(2,1)}, bf16[2,1024,256]{2,1,0:T(8,128)(2,1)}, u32[]{:S(2)}, u32[]{:S(2)}) collective-permute-start(bf16[2,1024,256]{2,1,0:T(8,128)(2,1)} %pad_maximum_fusion), channel_id=1, source_target_pairs={{0,4},{4,0},{8,12},{12,8},{16,20},{20,16},{24,28},{28,24},{32,36},... | collective-permute-start | bytes 3145736 | tf_op jit(solution)/shard_map/ppermute | solution.py:51
  52.8 8.4 %all-to-all-done = bf16[32,8,1152]{2,1,0:T(8,128)(2,1)S(1)} async-done(((bf16[32,8,1152]{2,1,0:T(8,128)(2,1)}), bf16[32,8,1152]{2,1,0:T(8,128)(2,1)S(1)}, u32[]{:S(2)}, u32[]{:S(2)}) %all-to-all-start) | async-done | bytes 589856 | tf_op jit(solution)/shard_map/all_to_all | solution.py:70
  62.8 1.2 fusion.30
  64.4 1.2 fusion.37
  67.1 1.2 fusion.43
  68.3 1.2 fusion.44
  69.6 1.2 fusion.45
  72.3 4.5 %all-to-all-start.1 = ((bf16[4,64,1536]{2,1,0:T(8,128)(2,1)}), bf16[4,64,1536]{2,1,0:T(8,128)(2,1)S(1)}, u32[]{:S(2)}, u32[]{:S(2)}) async-start(bf16[4,64,1536]{2,1,0:T(8,128)(2,1)} %bitcast.22), calls=%async_computation.1 | async-start | bytes 1572864 | tf_op jit(solution)/shard_map/all_to_all | solution.py:100
  77.0 10.4 %all-to-all-done.1 = bf16[4,64,1536]{2,1,0:T(8,128)(2,1)S(1)} async-done(((bf16[4,64,1536]{2,1,0:T(8,128)(2,1)}), bf16[4,64,1536]{2,1,0:T(8,128)(2,1)S(1)}, u32[]{:S(2)}, u32[]{:S(2)}) %all-to-all-start.1) | async-done | bytes 786464 | tf_op jit(solution)/shard_map/all_to_all | solution.py:100
  88.4 13.6 %all_gather.3 = bf16[256,1664]{1,0:T(8,128)(2,1)S(1)} all-gather(bf16[64,1664]{1,0:T(8,128)(2,1)S(1)} %concatenate.59), channel_id=1, replica_groups=mesh['ep'=128,'tp'=4] {'tp'}, dimensions={0}, use_global_device_ids=true | all-gather | bytes 1064960 | tf_op jit(solution)/shard_map/all_gather | solution.py:121
  111.0 1.4 convolution_add_fusion.3
  112.4 2.3 %maximum_maximum_fusion = bf16[2,1024,256]{2,1,0:T(8,128)(2,1)} fusion(bf16[1,512,256]{2,1,0:T(8,128)(2,1)} %fusion.8, bf16[1,512,256]{2,1,0:T(8,128)(2,1)} %fusion.7, bf16[1,512,256]{2,1,0:T(8,128)(2,1)} %fusion.6, bf16[1,512,256]{2,1,0:T(8,128)(2,1)} %fusion.5), kind=kLoop, calls=%fused_computation.30 | loop fusion | flops 4194304 | bytes 2097152 | tf_op jit(solution)/shard_map/stack | solution.py:152
  114.7 1.9 %collective-permute-start.4 = (bf16[2,1024,256]{2,1,0:T(8,128)(2,1)}, bf16[2,1024,256]{2,1,0:T(8,128)(2,1)}, u32[]{:S(2)}, u32[]{:S(2)}) collective-permute-start(bf16[2,1024,256]{2,1,0:T(8,128)(2,1)} %maximum_maximum_fusion), channel_id=1, source_target_pairs={{0,4},{4,0},{8,12},{12,8},{16,20},{20,16},{24,28},{28,24},{32,36},... | collective-permute-start | bytes 3145736 | tf_op jit(solution)/shard_map/ppermute | solution.py:154
  117.4 2.4 %collective-permute-start.6 = (bf16[2,256,512]{2,1,0:T(8,128)(2,1)}, bf16[2,256,512]{2,1,0:T(8,128)(2,1)}, u32[]{:S(2)}, u32[]{:S(2)}) collective-permute-start(bf16[2,256,512]{2,1,0:T(8,128)(2,1)} %pad_maximum_fusion.3), channel_id=1, source_target_pairs={{0,4},{4,0},{8,12},{12,8},{16,20},{20,16},{24,28},{28,24},{32,36},... | collective-permute-start | bytes 1572872 | tf_op jit(solution)/shard_map/ppermute | solution.py:155
  120.2 1.2 fusion.34
  121.4 1.2 convolution_add_fusion
  122.6 1.3 fusion.36
  123.9 1.2 fusion.4
  125.9 9.9 %all-to-all-start.2 = ((bf16[32,8,640]{2,1,0:T(8,128)(2,1)}), bf16[32,8,640]{2,1,0:T(8,128)(2,1)S(1)}, u32[]{:S(2)}, u32[]{:S(2)}) async-start(bf16[32,8,640]{2,1,0:T(8,128)(2,1)} %maximum_bitcast_fusion), calls=%async_computation.2 | async-start | bytes 655360 | tf_op jit(solution)/shard_map/all_to_all | solution.py:140
  137.2 1.9 %collective-permute-start.7 = (bf16[256,512]{1,0:T(8,128)(2,1)S(1)}, bf16[256,512]{1,0:T(8,128)(2,1)S(1)}, u32[]{:S(2)}, u32[]{:S(2)}) collective-permute-start(bf16[256,512]{1,0:T(8,128)(2,1)S(1)} %fusion.16), channel_id=1, source_target_pairs={{0,8},{4,12},{8,0},{12,4},{16,24},{20,28},{24,16},{28,20},{32,40},... | collective-permute-start | bytes 786440 | tf_op jit(solution)/shard_map/ppermute | solution.py:159
  139.7 7.1 %collective-permute-done.7 = bf16[256,512]{1,0:T(8,128)(2,1)S(1)} collective-permute-done((bf16[256,512]{1,0:T(8,128)(2,1)S(1)}, bf16[256,512]{1,0:T(8,128)(2,1)S(1)}, u32[]{:S(2)}, u32[]{:S(2)}) %collective-permute-start.7) | collective-permute-done | bytes 262176 | tf_op jit(solution)/shard_map/ppermute | solution.py:159
  147.7 1.4 convert_element_type.202
  150.1 2.2 %collective-permute-start.5 = (bf16[1024,256]{1,0:T(8,128)(2,1)}, bf16[1024,256]{1,0:T(8,128)(2,1)}, u32[]{:S(2)}, u32[]{:S(2)}) collective-permute-start(bf16[1024,256]{1,0:T(8,128)(2,1)} %fusion.12), channel_id=1, source_target_pairs={{0,8},{4,12},{8,0},{12,4},{16,24},{20,28},{24,16},{28,20},{32,40},... | collective-permute-start | bytes 1572872 | tf_op jit(solution)/shard_map/ppermute | solution.py:158
  152.3 8.1 %all-to-all-done.2 = bf16[32,8,640]{2,1,0:T(8,128)(2,1)S(1)} async-done(((bf16[32,8,640]{2,1,0:T(8,128)(2,1)}), bf16[32,8,640]{2,1,0:T(8,128)(2,1)S(1)}, u32[]{:S(2)}, u32[]{:S(2)}) %all-to-all-start.2) | async-done | bytes 327712 | tf_op jit(solution)/shard_map/all_to_all | solution.py:140
  162.3 2.4 %collective-permute-done.5 = bf16[1024,256]{1,0:T(8,128)(2,1)} collective-permute-done((bf16[1024,256]{1,0:T(8,128)(2,1)}, bf16[1024,256]{1,0:T(8,128)(2,1)}, u32[]{:S(2)}, u32[]{:S(2)}) %collective-permute-start.5) | collective-permute-done | bytes 524320 | tf_op jit(solution)/shard_map/ppermute | solution.py:158
  164.7 1.2 fusion.14
  (109 shorter events, 30.6 us)
Async XLA Ops:
  0.6 25.0 %copy-start.6 = (bf16[1,512,256]{2,1,0:T(8,128)(2,1)S(1)}, bf16[1,512,256]{2,1,0:T(8,128)(2,1)}, u32[]{:S(2)}) copy-start(bf16[1,512,256]{2,1,0:T(8,128)(2,1)} %param.12) | copy-start | bytes 786436
  0.6 25.0 %copy-start.7 = (bf16[1,512,256]{2,1,0:T(8,128)(2,1)S(1)}, bf16[1,512,256]{2,1,0:T(8,128)(2,1)}, u32[]{:S(2)}) copy-start(bf16[1,512,256]{2,1,0:T(8,128)(2,1)} %param.11) | copy-start | bytes 786436
  0.7 27.0 %copy-start.5 = (bf16[1,256,512]{2,1,0:T(8,128)(2,1)S(1)}, bf16[1,256,512]{2,1,0:T(8,128)(2,1)}, u32[]{:S(2)}) copy-start(bf16[1,256,512]{2,1,0:T(8,128)(2,1)} %param.13) | copy-start | bytes 786436
  5.5 41.7 %copy-start.8 = (s32[128]{0:T(128)}, s32[128]{0:T(128)S(1)}, u32[]{:S(2)}) copy-start(s32[128]{0:T(128)S(1)} %multiply_add_fusion) | copy-start | bytes 1540
  7.7 53.4 %all-to-all-start = ((bf16[32,8,1152]{2,1,0:T(8,128)(2,1)}), bf16[32,8,1152]{2,1,0:T(8,128)(2,1)S(1)}, u32[]{:S(2)}, u32[]{:S(2)}) async-start(bf16[32,8,1152]{2,1,0:T(8,128)(2,1)} %fusion), calls=%async_computation | async-start | bytes 1179648 | tf_op jit(solution)/shard_map/all_to_all | solution.py:70
  25.8 23.4 %collective-permute-start = (bf16[1024,256]{1,0:T(8,128)(2,1)S(1)}, bf16[1024,256]{1,0:T(8,128)(2,1)S(1)}, u32[]{:S(2)}, u32[]{:S(2)}) collective-permute-start(bf16[1024,256]{1,0:T(8,128)(2,1)S(1)} %get-tuple-element.46), channel_id=1, source_target_pairs={{0,8},{4,12},{8,0},{12,4},{16,24},{20,28},{24,16},{28,20},{32,40},... | collective-permute-start | bytes 1572872 | tf_op jit(solution)/shard_map/ppermute | solution.py:47
  27.7 18.7 %collective-permute-start.2 = (bf16[256,512]{1,0:T(8,128)(2,1)S(1)}, bf16[256,512]{1,0:T(8,128)(2,1)S(1)}, u32[]{:S(2)}, u32[]{:S(2)}) collective-permute-start(bf16[256,512]{1,0:T(8,128)(2,1)S(1)} %bitcast.169), channel_id=1, source_target_pairs={{0,8},{4,12},{8,0},{12,4},{16,24},{20,28},{24,16},{28,20},{32,40},... | collective-permute-start | bytes 786440 | tf_op jit(solution)/shard_map/ppermute | solution.py:48
  47.2 18.7 %collective-permute-start.3 = (bf16[2,256,512]{2,1,0:T(8,128)(2,1)}, bf16[2,256,512]{2,1,0:T(8,128)(2,1)}, u32[]{:S(2)}, u32[]{:S(2)}) collective-permute-start(bf16[2,256,512]{2,1,0:T(8,128)(2,1)} %pad_maximum_fusion.2), channel_id=1, source_target_pairs={{0,4},{4,0},{8,12},{12,8},{16,20},{20,16},{24,28},{28,24},{32,36},... | collective-permute-start | bytes 1572872 | tf_op jit(solution)/shard_map/ppermute | solution.py:52
  49.1 53.2 %copy-start.3 = (bf16[1024,256]{1,0:T(8,128)(2,1)}, bf16[1024,256]{1,0:T(8,128)(2,1)S(1)}, u32[]{:S(2)}) copy-start(bf16[1024,256]{1,0:T(8,128)(2,1)S(1)} %collective-permute-done) | copy-start | bytes 1572868
  50.4 12.4 %collective-permute-start.1 = (bf16[2,1024,256]{2,1,0:T(8,128)(2,1)}, bf16[2,1024,256]{2,1,0:T(8,128)(2,1)}, u32[]{:S(2)}, u32[]{:S(2)}) collective-permute-start(bf16[2,1024,256]{2,1,0:T(8,128)(2,1)} %pad_maximum_fusion), channel_id=1, source_target_pairs={{0,4},{4,0},{8,12},{12,8},{16,20},{20,16},{24,28},{28,24},{32,36},... | collective-permute-start | bytes 3145736 | tf_op jit(solution)/shard_map/ppermute | solution.py:51
  72.3 15.1 %all-to-all-start.1 = ((bf16[4,64,1536]{2,1,0:T(8,128)(2,1)}), bf16[4,64,1536]{2,1,0:T(8,128)(2,1)S(1)}, u32[]{:S(2)}, u32[]{:S(2)}) async-start(bf16[4,64,1536]{2,1,0:T(8,128)(2,1)} %bitcast.22), calls=%async_computation.1 | async-start | bytes 1572864 | tf_op jit(solution)/shard_map/all_to_all | solution.py:100
  102.0 2.5 %copy-start = (bf16[256,1664]{1,0:T(8,128)(2,1)}, bf16[256,1664]{1,0:T(8,128)(2,1)S(1)}, u32[]{:S(2)}) copy-start(bf16[256,1664]{1,0:T(8,128)(2,1)S(1)} %all_gather.3) | copy-start | bytes 2555908
  111.0 8.9 %copy-start.2 = (f32[256,512]{1,0:T(8,128)S(1)}, f32[256,512]{1,0:T(8,128)}, u32[]{:S(2)}) copy-start(f32[256,512]{1,0:T(8,128)} %fusion.38) | copy-start | bytes 1572868
  111.0 8.9 %copy-start.4 = (bf16[1024,256]{1,0:T(8,128)(2,1)S(1)}, bf16[1024,256]{1,0:T(8,128)(2,1)}, u32[]{:S(2)}) copy-start(bf16[1024,256]{1,0:T(8,128)(2,1)} %copy-done.3) | copy-start | bytes 1572868
  114.7 33.0 %collective-permute-start.4 = (bf16[2,1024,256]{2,1,0:T(8,128)(2,1)}, bf16[2,1024,256]{2,1,0:T(8,128)(2,1)}, u32[]{:S(2)}, u32[]{:S(2)}) collective-permute-start(bf16[2,1024,256]{2,1,0:T(8,128)(2,1)} %maximum_maximum_fusion), channel_id=1, source_target_pairs={{0,4},{4,0},{8,12},{12,8},{16,20},{20,16},{24,28},{28,24},{32,36},... | collective-permute-start | bytes 3145736 | tf_op jit(solution)/shard_map/ppermute | solution.py:154
  117.4 18.4 %collective-permute-start.6 = (bf16[2,256,512]{2,1,0:T(8,128)(2,1)}, bf16[2,256,512]{2,1,0:T(8,128)(2,1)}, u32[]{:S(2)}, u32[]{:S(2)}) collective-permute-start(bf16[2,256,512]{2,1,0:T(8,128)(2,1)} %pad_maximum_fusion.3), channel_id=1, source_target_pairs={{0,4},{4,0},{8,12},{12,8},{16,20},{20,16},{24,28},{28,24},{32,36},... | collective-permute-start | bytes 1572872 | tf_op jit(solution)/shard_map/ppermute | solution.py:155
  122.6 2.5 %slice-start = ((bf16[256,1664]{1,0:T(8,128)(2,1)}), bf16[256,128]{1,0:T(8,128)(2,1)S(1)}, s32[]{:S(2)}) async-start(bf16[256,1664]{1,0:T(8,128)(2,1)} %copy-done), calls=%async_computation.3 | async-start | bytes 131072 | tf_op jit(solution)/shard_map/slice | solution.py:138
  125.9 34.5 %all-to-all-start.2 = ((bf16[32,8,640]{2,1,0:T(8,128)(2,1)}), bf16[32,8,640]{2,1,0:T(8,128)(2,1)S(1)}, u32[]{:S(2)}, u32[]{:S(2)}) async-start(bf16[32,8,640]{2,1,0:T(8,128)(2,1)} %maximum_bitcast_fusion), calls=%async_computation.2 | async-start | bytes 655360 | tf_op jit(solution)/shard_map/all_to_all | solution.py:140
  137.2 9.6 %collective-permute-start.7 = (bf16[256,512]{1,0:T(8,128)(2,1)S(1)}, bf16[256,512]{1,0:T(8,128)(2,1)S(1)}, u32[]{:S(2)}, u32[]{:S(2)}) collective-permute-start(bf16[256,512]{1,0:T(8,128)(2,1)S(1)} %fusion.16), channel_id=1, source_target_pairs={{0,8},{4,12},{8,0},{12,4},{16,24},{20,28},{24,16},{28,20},{32,40},... | collective-permute-start | bytes 786440 | tf_op jit(solution)/shard_map/ppermute | solution.py:159
  139.7 9.4 %copy-start.1 = (f32[512,256]{1,0:T(8,128)S(1)}, f32[512,256]{1,0:T(8,128)}, u32[]{:S(2)}) copy-start(f32[512,256]{1,0:T(8,128)} %fusion.94) | copy-start | bytes 1572868
  149.1 11.2 %copy-start.9 = (s32[128]{0:T(128)S(1)}, s32[128]{0:T(128)}, u32[]{:S(2)}) copy-start(s32[128]{0:T(128)} %copy-done.8) | copy-start | bytes 1540
  150.1 14.6 %collective-permute-start.5 = (bf16[1024,256]{1,0:T(8,128)(2,1)}, bf16[1024,256]{1,0:T(8,128)(2,1)}, u32[]{:S(2)}, u32[]{:S(2)}) collective-permute-start(bf16[1024,256]{1,0:T(8,128)(2,1)} %fusion.12), channel_id=1, source_target_pairs={{0,8},{4,12},{8,0},{12,4},{16,24},{20,28},{24,16},{28,20},{32,40},... | collective-permute-start | bytes 1572872 | tf_op jit(solution)/shard_map/ppermute | solution.py:158

commit v2 on v1

v2 whole, which is shorter than its diff:
```python
import jax
import jax.numpy as jnp
from jax import lax
from jax.experimental import pallas as pl
from jax.experimental.pallas import tpu as pltpu
from jax.sharding import PartitionSpec as P

BF = jnp.bfloat16
F32 = jnp.float32
I32 = jnp.int32
GROUP = 4
CAP = 8
LANES = 128
ORDER = (0, 2, 1, 3)


def exchange_groups(peers):
    planes = peers // 8
    groups = []
    for low in (0, 1):
        for core in (0, 1):
            groups.append([z * 8 + x * 2 + core for x in (low, 3 - low) for z in range(planes)])
    return groups


def partner(peers, bit):
    return [(i, i ^ bit) for i in range(peers)]


def dot(a, b, ca, cb):
    return lax.dot_general(a, b, (((ca,), (cb,)), ((), ())), preferred_element_type=F32)


def iota(shape, dim):
    return lax.broadcasted_iota(I32, shape, dim)


def call(kernel, outs, *args, **kwargs):
    return pl.pallas_call(
        kernel,
        out_shape=outs,
        compiler_params=pltpu.CompilerParams(vmem_limit_bytes=20 * 1024 * 1024),
        **kwargs,
    )(*args)


def shape(dims, dtype):
    return jax.ShapeDtypeStruct(dims, dtype)


def placement(experts, n_groups):
    toks = experts.shape[1]
    group = lax.shift_right_logical(experts[0:1, :], 2)
    group = (group & 1) * (n_groups // 2) + lax.shift_right_logical(group, 1)
    member = iota((n_groups, toks), 0) == group
    onehot = jnp.where(member, 1.0, 0.0)
    earlier = jnp.where(iota((toks, toks), 0) < iota((toks, toks), 1), 1.0, 0.0).astype(BF)
    cum = dot(onehot.astype(BF), earlier, 1, 0)
    pos = jnp.sum(onehot * cum, axis=0, keepdims=True).astype(I32)
    slot = group * CAP + pos
    return jnp.where(iota((n_groups * CAP, toks), 0) == slot, 1.0, 0.0).astype(BF)


def send_kernel(tok_hbm, cot_hbm, exp_hbm, comb_hbm, out_ref, tok_ref, cot_ref, exp_ref, comb_ref, sems):
    copies = [
        pltpu.make_async_copy(src, dst, sems.at[i])
        for i, (src, dst) in enumerate(
            ((exp_hbm, exp_ref), (comb_hbm, comb_ref), (tok_hbm, tok_ref), (cot_hbm, cot_ref))
        )
    ]
    for copy in copies:
        copy.start()
    for copy in copies:
        copy.wait()
    block = tok_ref.shape[1]
    toks = tok_ref.shape[0]
    n_groups = out_ref.shape[0] // CAP
    experts = exp_ref[...]
    place = placement(experts, n_groups)
    local = experts & (GROUP - 1)
    weight = comb_ref[...].astype(BF).astype(F32)
    row = iota((LANES, toks), 0)
    meta = jnp.where(row == local[0:1, :], weight[0:1, :], 0.0) + jnp.where(
        row == local[1:2, :], weight[1:2, :], 0.0
    )
    out_ref[:, :block] = dot(place, tok_ref[...], 1, 0).astype(BF)
    out_ref[:, block : 2 * block] = dot(place, cot_ref[...], 1, 0).astype(BF)
    out_ref[:, 2 * block :] = dot(place, meta.astype(BF), 1, 1).astype(BF)


def chosen(meta):
    lane = iota(meta.shape, 1)
    used = meta > 0
    first = jnp.min(jnp.where(used, lane, 99), axis=1, keepdims=True)
    second = jnp.max(jnp.where(used, lane, -1), axis=1, keepdims=True)
    return first, second


def picks(meta, hidden):
    first, second = chosen(meta)
    wide = (meta.shape[0], hidden)
    return jnp.broadcast_to(first, wide), jnp.broadcast_to(second, wide)


def weights(w_refs, r, rows):
    return w_refs[r][rows, :]


def parts_kernel(arr_ref, own_ref, sib_ref, x_ref, xsib_ref, out_ref):
    w_refs = (own_ref, sib_ref, x_ref, xsib_ref)
    hidden = own_ref.shape[1]
    block = own_ref.shape[0] // 6 * 2
    mine = lax.axis_index("ep") & (GROUP - 1)
    first, second = picks(arr_ref[:, 2 * block :].astype(F32), hidden)
    rows = arr_ref[:, :block]
    for q in range(3):
        p0 = jnp.zeros(first.shape, F32)
        p1 = p0
        for r in ORDER:
            if q < 2:
                dense = dot(rows, weights(w_refs, r, slice(q * block, (q + 1) * block)), 1, 0)
            else:
                half = block // 2
                dense = dot(
                    arr_ref[:, block : block + half],
                    weights(w_refs, r, slice(2 * block, 2 * block + half)),
                    1,
                    1,
                ) + dot(
                    arr_ref[:, block + half : 2 * block],
                    weights(w_refs, r, slice(2 * block + half, 3 * block)),
                    1,
                    1,
                )
            expert = mine ^ r
            p0 = jnp.where(first == expert, dense, p0)
            p1 = jnp.where(second == expert, dense, p1)
        out_ref[:, q * hidden : (q + 1) * hidden] = p0.astype(BF)
        out_ref[:, (3 + q) * hidden : (4 + q) * hidden] = p1.astype(BF)


def act_kernel(part_ref, arr_ref, out_ref):
    share = part_ref.shape[1]
    hidden = part_ref.shape[2] // 6
    meta_at = arr_ref.shape[1] - LANES
    me = lax.axis_index("tp")
    meta = arr_ref[pl.ds(pl.multiple_of(me * share, share), share), meta_at:].astype(F32)
    first, second = chosen(meta)
    lane = iota((share, LANES), 1)
    extra = jnp.zeros((share, LANES), F32)
    for k, pick in enumerate((first, second)):
        weight = jnp.sum(jnp.where(lane == pick, meta, 0.0), axis=1, keepdims=True)
        total = []
        for q in range(3):
            at = slice((3 * k + q) * hidden, (3 * k + q + 1) * hidden)
            acc = part_ref[0, :, at].astype(F32)
            for d in range(1, part_ref.shape[0]):
                acc = acc + part_ref[d, :, at].astype(F32)
            total.append(acc)
        gate_pre, up_pre, grad_scaled = total
        sig = jax.nn.sigmoid(gate_pre)
        silu = gate_pre * sig
        hid = silu * up_pre
        gh = weight * grad_scaled
        at = 3 * k * hidden
        out_ref[:, at : at + hidden] = (weight * hid).astype(BF)
        out_ref[:, at + hidden : at + 2 * hidden] = (
            gh * up_pre * sig * (1.0 + gate_pre * (1.0 - sig))
        ).astype(BF)
        out_ref[:, at + 2 * hidden : at + 3 * hidden] = (gh * silu).astype(BF)
        comb = jnp.sum(hid * grad_scaled, axis=1, keepdims=True)
        high = comb.astype(BF).astype(F32)
        extra = jnp.where(lane == 2 * k, high, jnp.where(lane == 2 * k + 1, comb - high, extra))
    out_ref[:, 6 * hidden :] = extra.astype(BF)


def masks(arr_ref, hidden):
    mine = lax.axis_index("ep") & (GROUP - 1)
    meta = arr_ref[:, arr_ref.shape[1] - LANES :].astype(F32)
    first, second = picks(meta, hidden)
    out = {}
    for r in ORDER:
        expert = mine ^ r
        out[r] = tuple(jnp.where(p == expert, 1.0, 0.0).astype(BF) for p in (first, second))
    return out


def spread(act_ref, mask, q, hidden):
    return (
        act_ref[:, q * hidden : (q + 1) * hidden] * mask[0]
        + act_ref[:, (3 + q) * hidden : (4 + q) * hidden] * mask[1]
    )


def back_kernel(act_ref, arr_ref, own_ref, sib_ref, x_ref, xsib_ref, out_ref):
    w_refs = (own_ref, sib_ref, x_ref, xsib_ref)
    hidden = own_ref.shape[1]
    block = own_ref.shape[0] // 6 * 2
    mask = masks(arr_ref, hidden)
    acc = jnp.zeros((act_ref.shape[0], block), F32)
    for r in ORDER:
        for q in (1, 2):
            w = weights(w_refs, r, slice((q - 1) * block, q * block))
            acc = acc + dot(spread(act_ref, mask[r], q, hidden), w, 1, 1)
    out_ref[:, :block] = acc.astype(BF)
    out_ref[:, block:] = act_ref[:, 6 * hidden :]


def stacked(block):
    half = block // 2
    return (
        slice(0, block),
        slice(block, 2 * block),
        slice(2 * block, 2 * block + half),
        slice(2 * block + half, 3 * block),
    )


def grads_kernel(act_ref, arr_ref, send_ref, pass_ref, keep_ref):
    hidden = send_ref.shape[2]
    block = send_ref.shape[1] // 3
    g, u, d0, d1 = stacked(block)
    mask = masks(arr_ref, hidden)
    rows = arr_ref[:, :block]
    cots = arr_ref[:, block : 2 * block]
    for r, ref in ((1, send_ref.at[0]), (3, send_ref.at[1]), (2, pass_ref), (0, keep_ref)):
        ref[g, :] = dot(rows, spread(act_ref, mask[r], 1, hidden), 0, 0).astype(BF)
        ref[u, :] = dot(rows, spread(act_ref, mask[r], 2, hidden), 0, 0).astype(BF)
        down = dot(spread(act_ref, mask[r], 0, hidden), cots, 0, 0).astype(BF)
        ref[d0, :] = down[:, : block // 2]
        ref[d1, :] = down[:, block // 2 :]


def half_kernel(pass_ref, got_ref, out_ref):
    out_ref[...] = (pass_ref[...].astype(F32) + got_ref[1].astype(F32)).astype(BF)


def total_kernel(keep_ref, got_ref, last_ref, gate_ref, up_ref, down_ref):
    block = gate_ref.shape[0]
    g, u, d0, d1 = stacked(block)

    def total(at):
        return keep_ref[at, :].astype(F32) + got_ref[0, at, :].astype(F32) + last_ref[at, :].astype(F32)

    gate_ref[...] = total(g)
    up_ref[...] = total(u)
    down_ref[:, : block // 2] = total(d0)
    down_ref[:, block // 2 :] = total(d1)


def final_kernel(ret_ref, exp_ref, tok_ref, comb_ref):
    block = tok_ref.shape[1]
    experts = exp_ref[...]
    place = placement(experts, ret_ref.shape[0] // CAP)
    tok_ref[...] = dot(place, ret_ref[:, :block], 0, 0).astype(BF)
    extra = dot(ret_ref[:, block:], place, 0, 0)
    low = extra[0:1, :] + extra[1:2, :]
    high = extra[2:3, :] + extra[3:4, :]
    rising = experts[0:1, :] < experts[1:2, :]
    comb_ref[0:1, :] = jnp.where(rising, low, high)
    comb_ref[1:2, :] = jnp.where(rising, high, low)


def body(tokens, cotangent, experts, combine, w_gate, w_up, w_down):
    peers = lax.axis_size("ep")
    widths = lax.axis_size("tp")
    toks, block = tokens.shape
    hidden = w_gate.shape[2]
    n_groups = peers // GROUP
    slots = n_groups * CAP
    share = slots // widths
    groups = exchange_groups(peers)
    half = block // 2

    sources = (tokens, cotangent, experts.T, combine.T)
    payload = call(
        send_kernel,
        shape((slots, 2 * block + LANES), BF),
        *(pltpu.with_memory_space_constraint(a, pltpu.HBM) for a in sources),
        in_specs=[pl.BlockSpec(memory_space=pltpu.HBM)] * 4,
        scratch_shapes=[pltpu.VMEM(a.shape, a.dtype) for a in sources]
        + [pltpu.SemaphoreType.DMA((4,))],
    )
    arrived = lax.all_to_all(
        payload.reshape(n_groups, CAP, -1),
        "ep",
        split_axis=0,
        concat_axis=0,
        tiled=True,
        axis_index_groups=groups,
    ).reshape(slots, -1)
    arrived = pltpu.with_memory_space_constraint(arrived, pltpu.VMEM)
    own = jnp.concatenate([w_gate[0], w_up[0], w_down[0][:, :half], w_down[0][:, half:]], axis=0)
    other = lax.ppermute(own, "ep", partner(peers, 2))
    sibling = lax.ppermute(own, "ep", partner(peers, 1))
    across = lax.ppermute(other, "ep", partner(peers, 1))
    w_all = tuple(
        pltpu.with_memory_space_constraint(w, pltpu.VMEM) for w in (own, sibling, other, across)
    )
    parts = call(parts_kernel, shape((slots, 6 * hidden), BF), arrived, *w_all)
    pieces = lax.all_to_all(
        parts.reshape(widths, share, -1), "tp", split_axis=0, concat_axis=0, tiled=True
    )
    acts = call(act_kernel, shape((share, 6 * hidden + LANES), BF), pieces, arrived)
    acts = lax.all_gather(acts, "tp", axis=0, tiled=True)
    acts = pltpu.with_memory_space_constraint(acts, pltpu.VMEM)
    back = call(back_kernel, shape((slots, block + LANES), BF), acts, arrived, *w_all)
    returned = lax.all_to_all(
        back.reshape(n_groups, CAP, -1),
        "ep",
        split_axis=0,
        concat_axis=0,
        tiled=True,
        axis_index_groups=groups,
    ).reshape(slots, -1)
    stack = (3 * block, hidden)
    send, through, keep = call(
        grads_kernel, (shape((2, *stack), BF), shape(stack, BF), shape(stack, BF)), acts, arrived
    )
    got = lax.ppermute(send, "ep", partner(peers, 1))
    pair = call(half_kernel, shape(stack, BF), through, got)
    last = lax.ppermute(pair, "ep", partner(peers, 2))
    gate_grad, up_grad, down_grad = call(
        total_kernel,
        (shape((block, hidden), F32), shape((block, hidden), F32), shape((hidden, block), F32)),
        keep,
        got,
        last,
    )
    grad_tokens, comb = call(
        final_kernel, (shape((toks, block), BF), shape((2, toks), F32)), returned, experts.T
    )
    return (grad_tokens, comb.T, gate_grad[None], up_grad[None], down_grad[None])


def solution(mesh):
    return jax.shard_map(
        body,
        mesh=mesh,
        in_specs=(
            P("ep", "tp"),
            P("ep", "tp"),
            P("ep", None),
            P("ep", None),
            P("ep", "tp", None),
            P("ep", "tp", None),
            P("ep", None, "tp"),
        ),
        out_specs=(
            P("ep", "tp"),
            P("ep", None),
            P("ep", "tp", None),
            P("ep", "tp", None),
            P("ep", None, "tp"),
        ),
        check_vma=False,
    )
```

time: 168 us -> 130 us (0.77)
  matrix products: 26.8 us -> 0 us
  other arithmetic: 17.7 us -> 0.05 us
  blocking collectives: 13.6 us -> 30 us
  starting transfers between devices: 50.9 us -> 36.5 us
  Pallas kernels: 0 us -> 12 us
  waiting for transfers between devices: 51.1 us -> 45.6 us
  local copies, waits for them, and re-layouts: 5.56 us -> 3.23 us
    dot_general x34 -> x0, matrix products: 26.8 us -> none  [dot(): lax.dot_general(a, b, (contract, ((), ())), preferred_element_type=F32)]
    all_to_all x0 -> x1, blocking collectives: none -> 16.1 us  [body(): lax.all_to_all(parts.reshape(widths, share, -1), 'tp', split_axis=0, conc...]
    pallas_call x0 -> x8, Pallas kernels: none -> 12 us  [call(): pl.pallas_call(kernel, out_shape=outs, compiler_params=pltpu.CompilerPara...]
    ppermute x8 -> x5, starting transfers between devices: 18.6 us -> 9.57 us  [the longest x1 1.92 us: body(): other = lax.ppermute(own, 'ep', partner(peers, 2))]
    another operation x6 -> x0, other arithmetic: 5.42 us -> none  [the longest x1 2.29 us: body(): jnp.stack([jnp.concatenate(part[r][:2]).astype(BF) for r in (2, 3)])]
    all_to_all x3 -> x2, starting transfers between devices: 32.3 us -> 27 us  [the longest x1 17.9 us: body(): lax.all_to_all(payload.reshape(n_groups, CAP, -1), 'ep', split_axis=0, co...]
    ppermute x8 -> x5, waiting for transfers between devices: 24.3 us -> 19 us  [the longest x1 16.8 us: body(): other = lax.ppermute(own, 'ep', partner(peers, 2))]
    convert_element_type x10 -> x0, other arithmetic: 4.28 us -> none  [the longest x1 1.38 us: body(): got_gu = lax.ppermute(sib_gu, 'ep', partner(peers, 1)).astype(F32)]
  transfers between devices with their start and end apart: 11 -> 7, of which waited for: 6 -> 4; matrix products, arithmetic and copies ran while one was open for 13% -> 0% of each run, Pallas kernels for 0% -> 3%
where the time goes in v2:
time: 130 us; the launch traced here: 128 us
  waiting for transfers between devices  45.6 us (35%)
  starting transfers between devices  36.5 us (28%)
  blocking collectives  30 us (23%)
  Pallas kernels  12 us (9%)
  local copies, waits for them, and re-layouts  3.23 us (2%)
    all_to_all x1, waiting for transfers between devices, body(): lax.all_to_all(back.reshape(n_groups, CAP, -1), 'ep', split_axis=0, conca...  19.9 us
    all_to_all x1, starting transfers between devices, body(): lax.all_to_all(payload.reshape(n_groups, CAP, -1), 'ep', split_axis=0, co...  17.9 us
    ppermute x1, waiting for transfers between devices, body(): other = lax.ppermute(own, 'ep', partner(peers, 2))  16.8 us
    all_to_all x1, blocking collectives, body(): lax.all_to_all(parts.reshape(widths, share, -1), 'tp', split_axis=0, conc...  16.1 us
    all_gather x1, blocking collectives, body(): acts = lax.all_gather(acts, 'tp', axis=0, tiled=True)  13.9 us
    pallas_call x8, Pallas kernels, call(): pl.pallas_call(kernel, out_shape=outs, compiler_params=pltpu.CompilerPara...  12 us
    all_to_all x1, starting transfers between devices, body(): lax.all_to_all(back.reshape(n_groups, CAP, -1), 'ep', split_axis=0, conca...  9.04 us
    all_to_all x1, waiting for transfers between devices, body(): lax.all_to_all(payload.reshape(n_groups, CAP, -1), 'ep', split_axis=0, co...  6.64 us
  transfers between devices with their start and end apart: 7, of which 4 were waited for; matrix products, arithmetic and copies ran while one was open for 0% of the time, Pallas kernels for 3%

profile of v2, /device:TPU:6, one launch (start us, length us, event | category | flops | bytes accessed | tf_op | source)
XLA Modules:
  0.0 128.3 jit_solution(2137657289777793319)
XLA Ops:
  0.6 0.0 copy-start.12
  0.6 0.0 copy-start.13
  0.7 0.0 copy-start.14
  0.7 2.4 %shard_map.110 = bf16[256,1152]{1,0:T(8,128)(2,1)} custom-call(bf16[128,512]{1,0:T(8,128)(2,1)} %tok_hbm.1, bf16[128,512]{1,0:T(8,128)(2,1)} %cot_hbm.1, s32[2,128]{1,0:T(2,128)} %bitcast.20, f32[2,128]{1,0:T(2,128)} %bitcast.25), custom_call_target="tpu_custom_call" | custom-call | tf_op jit(solution)/shard_map/pallas_call | solution.py:39
  3.1 17.9 %all-to-all-start = ((bf16[32,8,1152]{2,1,0:T(8,128)(2,1)}), bf16[32,8,1152]{2,1,0:T(8,128)(2,1)S(1)}, u32[]{:S(2)}, u32[]{:S(2)}) async-start(bf16[32,8,1152]{2,1,0:T(8,128)(2,1)} %bitcast.2), calls=%async_computation | async-start | bytes 1179648 | tf_op jit(solution)/shard_map/all_to_all | solution.py:284
  21.0 0.0 copy-done.12
  21.1 0.1 pad_maximum_fusion.own_ref
  21.1 1.9 %collective-permute-start.1 = (bf16[1536,256]{1,0:T(8,128)(2,1)S(1)}, bf16[1536,256]{1,0:T(8,128)(2,1)S(1)}, u32[]{:S(2)}, u32[]{:S(2)}) collective-permute-start(bf16[1536,256]{1,0:T(8,128)(2,1)S(1)} %pad_maximum_fusion.own_ref), channel_id=1, source_target_pairs={{0,8},{4,12},{8,0},{12,4},{16,24},{20,28},{24,16},{28,20},{32,40},... | collective-permute-start | bytes 2359304 | tf_op jit(solution)/shard_map/ppermute | solution.py:294
  23.1 1.9 %collective-permute-start = (bf16[1536,256]{1,0:T(8,128)(2,1)S(1)}, bf16[1536,256]{1,0:T(8,128)(2,1)S(1)}, u32[]{:S(2)}, u32[]{:S(2)}) collective-permute-start(bf16[1536,256]{1,0:T(8,128)(2,1)S(1)} %pad_maximum_fusion.own_ref), channel_id=1, source_target_pairs={{0,4},{4,0},{8,12},{12,8},{16,20},{20,16},{24,28},{28,24},{32,36},... | collective-permute-start | bytes 2359304 | tf_op jit(solution)/shard_map/ppermute | solution.py:295
  25.0 16.8 %collective-permute-done.1.x_ref = bf16[1536,256]{1,0:T(8,128)(2,1)S(1)} collective-permute-done((bf16[1536,256]{1,0:T(8,128)(2,1)S(1)}, bf16[1536,256]{1,0:T(8,128)(2,1)S(1)}, u32[]{:S(2)}, u32[]{:S(2)}) %collective-permute-start.1) | collective-permute-done | bytes 786464 | tf_op jit(solution)/shard_map/ppermute | solution.py:294
  41.7 1.9 %collective-permute-start.2 = (bf16[1536,256]{1,0:T(8,128)(2,1)S(1)}, bf16[1536,256]{1,0:T(8,128)(2,1)S(1)}, u32[]{:S(2)}, u32[]{:S(2)}) collective-permute-start(bf16[1536,256]{1,0:T(8,128)(2,1)S(1)} %collective-permute-done.1.x_ref), channel_id=1, source_target_pairs={{0,4},{4,0},{8,12},{12,8},{16,20},{20,16},{24,28},{28,24},{32,36},... | collective-permute-start | bytes 2359304 | tf_op jit(solution)/shard_map/ppermute | solution.py:296
  43.7 0.0 collective-permute-done.sib_ref
  43.7 2.2 %collective-permute-done.2.xsib_ref = bf16[1536,256]{1,0:T(8,128)(2,1)S(1)} collective-permute-done((bf16[1536,256]{1,0:T(8,128)(2,1)S(1)}, bf16[1536,256]{1,0:T(8,128)(2,1)S(1)}, u32[]{:S(2)}, u32[]{:S(2)}) %collective-permute-start.2) | collective-permute-done | bytes 786464 | tf_op jit(solution)/shard_map/ppermute | solution.py:296
  45.9 0.9 copy-done.4
  46.8 6.6 %all-to-all-done = bf16[32,8,1152]{2,1,0:T(8,128)(2,1)S(1)} async-done(((bf16[32,8,1152]{2,1,0:T(8,128)(2,1)}), bf16[32,8,1152]{2,1,0:T(8,128)(2,1)S(1)}, u32[]{:S(2)}, u32[]{:S(2)}) %all-to-all-start) | async-done | bytes 589856 | tf_op jit(solution)/shard_map/all_to_all | solution.py:284
  53.5 1.1 copy-done.5
  54.6 1.0 shard_map.111
  55.7 16.1 %all_to_all.15.part_ref = bf16[4,64,1536]{2,1,0:T(8,128)(2,1)S(1)} all-to-all(bf16[4,64,1536]{2,1,0:T(8,128)(2,1)S(1)} %bitcast.18), channel_id=1, replica_groups=mesh['ep'=128,'tp'=4] {'tp'}, dimensions={0} | all-to-all | bytes 1572864 | tf_op jit(solution)/shard_map/all_to_all | solution.py:301
  71.8 0.3 shard_map.112
  72.1 13.9 %all_gather.3.act_ref = bf16[256,1664]{1,0:T(8,128)(2,1)S(1)} all-gather(bf16[64,1664]{1,0:T(8,128)(2,1)S(1)} %shard_map.112), channel_id=1, replica_groups=mesh['ep'=128,'tp'=4] {'tp'}, dimensions={0}, use_global_device_ids=true | all-gather | bytes 1064960 | tf_op jit(solution)/shard_map/all_gather | solution.py:305
  86.0 2.1 %shard_map.115 = (bf16[2,1536,256]{2,1,0:T(8,128)(2,1)}, bf16[1536,256]{1,0:T(8,128)(2,1)S(1)}, bf16[1536,256]{1,0:T(8,128)(2,1)S(1)}) custom-call(bf16[256,1664]{1,0:T(8,128)(2,1)S(1)} %all_gather.3.act_ref, bf16[256,1152]{1,0:T(8,128)(2,1)S(1)} %bitcast.16), custom_call_target="tpu_custom_call" | custom-call | tf_op jit(solution)/shard_map/pallas_call | solution.py:39
  88.1 1.9 %collective-permute-start.3 = (bf16[2,1536,256]{2,1,0:T(8,128)(2,1)}, bf16[2,1536,256]{2,1,0:T(8,128)(2,1)S(1)}, u32[]{:S(2)}, u32[]{:S(2)}) collective-permute-start(bf16[2,1536,256]{2,1,0:T(8,128)(2,1)} %get-tuple-element.16), channel_id=1, source_target_pairs={{0,4},{4,0},{8,12},{12,8},{16,20},{20,16},{24,28},{28,24},{32,36},... | collective-permute-start | bytes 4718600 | tf_op jit(solution)/shard_map/ppermute | solution.py:320
  90.1 1.7 %shard_map.113 = bf16[256,640]{1,0:T(8,128)(2,1)} custom-call(bf16[256,1664]{1,0:T(8,128)(2,1)S(1)} %all_gather.3.act_ref, bf16[256,1152]{1,0:T(8,128)(2,1)S(1)} %bitcast.17, bf16[1536,256]{1,0:T(8,128)(2,1)S(1)} %pad_maximum_fusion.own_ref, bf16[1536,256]{1,0:T(8,128)(2,1)S(1)} %copy-done.3, bf16[1536,256]{1,0:T(8,128)(2,1)S(1)} %copy-done.1, ...), custom_call_target="tpu_custom_call" | custom-call | tf_op jit(solution)/shard_map/pallas_call | solution.py:39
  91.8 9.0 %all-to-all-start.2 = ((bf16[32,8,640]{2,1,0:T(8,128)(2,1)}), bf16[32,8,640]{2,1,0:T(8,128)(2,1)S(1)}, u32[]{:S(2)}, u32[]{:S(2)}) async-start(bf16[32,8,640]{2,1,0:T(8,128)(2,1)} %bitcast.8), calls=%async_computation.2 | async-start | bytes 655360 | tf_op jit(solution)/shard_map/all_to_all | solution.py:308
  100.8 0.0 collective-permute-done.3.got_ref
  100.8 1.1 copy-done.10
  102.0 1.1 shard_map.116
  103.1 1.9 %collective-permute-start.4 = (bf16[1536,256]{1,0:T(8,128)(2,1)}, bf16[1536,256]{1,0:T(8,128)(2,1)}, u32[]{:S(2)}, u32[]{:S(2)}) collective-permute-start(bf16[1536,256]{1,0:T(8,128)(2,1)} %shard_map.116), channel_id=1, source_target_pairs={{0,8},{4,12},{8,0},{12,4},{16,24},{20,28},{24,16},{28,20},{32,40},... | collective-permute-start | bytes 2359304 | tf_op jit(solution)/shard_map/ppermute | solution.py:322
  105.0 19.9 %all-to-all-done.2 = bf16[32,8,640]{2,1,0:T(8,128)(2,1)S(1)} async-done(((bf16[32,8,640]{2,1,0:T(8,128)(2,1)}), bf16[32,8,640]{2,1,0:T(8,128)(2,1)S(1)}, u32[]{:S(2)}, u32[]{:S(2)}) %all-to-all-start.2) | async-done | bytes 327712 | tf_op jit(solution)/shard_map/all_to_all | solution.py:308
  124.9 1.0 shard_map.114
  125.9 0.0 collective-permute-done.4.last_ref
  126.0 2.4 %shard_map.117 = (f32[512,256]{1,0:T(8,128)}, f32[512,256]{1,0:T(8,128)}, f32[256,512]{1,0:T(8,128)}) custom-call(bf16[1536,256]{1,0:T(8,128)(2,1)S(1)} %copy-done.8, bf16[2,1536,256]{2,1,0:T(8,128)(2,1)S(1)} %collective-permute-done.3.got_ref, bf16[1536,256]{1,0:T(8,128)(2,1)} %collective-permute-done.4.last_ref), custom_call_target="tpu_custom_call" | custom-call | tf_op jit(solution)/shard_map/pallas_call | solution.py:39
  (24 shorter events, 0.1 us)
Async XLA Ops:
  0.6 20.4 %copy-start.12 = (bf16[1,256,512]{2,1,0:T(8,128)(2,1)S(1)}, bf16[1,256,512]{2,1,0:T(8,128)(2,1)}, u32[]{:S(2)}) copy-start(bf16[1,256,512]{2,1,0:T(8,128)(2,1)} %param.13) | copy-start | bytes 786436
  0.6 20.4 %copy-start.13 = (bf16[1,512,256]{2,1,0:T(8,128)(2,1)S(1)}, bf16[1,512,256]{2,1,0:T(8,128)(2,1)}, u32[]{:S(2)}) copy-start(bf16[1,512,256]{2,1,0:T(8,128)(2,1)} %param.12) | copy-start | bytes 786436
  0.7 20.4 %copy-start.14 = (bf16[1,512,256]{2,1,0:T(8,128)(2,1)S(1)}, bf16[1,512,256]{2,1,0:T(8,128)(2,1)}, u32[]{:S(2)}) copy-start(bf16[1,512,256]{2,1,0:T(8,128)(2,1)} %param.11) | copy-start | bytes 786436
  3.1 50.4 %all-to-all-start = ((bf16[32,8,1152]{2,1,0:T(8,128)(2,1)}), bf16[32,8,1152]{2,1,0:T(8,128)(2,1)S(1)}, u32[]{:S(2)}, u32[]{:S(2)}) async-start(bf16[32,8,1152]{2,1,0:T(8,128)(2,1)} %bitcast.2), calls=%async_computation | async-start | bytes 1179648 | tf_op jit(solution)/shard_map/all_to_all | solution.py:284
  21.1 20.6 %collective-permute-start.1 = (bf16[1536,256]{1,0:T(8,128)(2,1)S(1)}, bf16[1536,256]{1,0:T(8,128)(2,1)S(1)}, u32[]{:S(2)}, u32[]{:S(2)}) collective-permute-start(bf16[1536,256]{1,0:T(8,128)(2,1)S(1)} %pad_maximum_fusion.own_ref), channel_id=1, source_target_pairs={{0,8},{4,12},{8,0},{12,4},{16,24},{20,28},{24,16},{28,20},{32,40},... | collective-permute-start | bytes 2359304 | tf_op jit(solution)/shard_map/ppermute | solution.py:294
  23.1 20.6 %collective-permute-start = (bf16[1536,256]{1,0:T(8,128)(2,1)S(1)}, bf16[1536,256]{1,0:T(8,128)(2,1)S(1)}, u32[]{:S(2)}, u32[]{:S(2)}) collective-permute-start(bf16[1536,256]{1,0:T(8,128)(2,1)S(1)} %pad_maximum_fusion.own_ref), channel_id=1, source_target_pairs={{0,4},{4,0},{8,12},{12,8},{16,20},{20,16},{24,28},{28,24},{32,36},... | collective-permute-start | bytes 2359304 | tf_op jit(solution)/shard_map/ppermute | solution.py:295
  41.7 13.9 %copy-start = (bf16[1536,256]{1,0:T(8,128)(2,1)}, bf16[1536,256]{1,0:T(8,128)(2,1)S(1)}, u32[]{:S(2)}) copy-start(bf16[1536,256]{1,0:T(8,128)(2,1)S(1)} %collective-permute-done.1.x_ref) | copy-start | bytes 2359300
  41.7 4.2 %collective-permute-start.2 = (bf16[1536,256]{1,0:T(8,128)(2,1)S(1)}, bf16[1536,256]{1,0:T(8,128)(2,1)S(1)}, u32[]{:S(2)}, u32[]{:S(2)}) collective-permute-start(bf16[1536,256]{1,0:T(8,128)(2,1)S(1)} %collective-permute-done.1.x_ref), channel_id=1, source_target_pairs={{0,4},{4,0},{8,12},{12,8},{16,20},{20,16},{24,28},{28,24},{32,36},... | collective-permute-start | bytes 2359304 | tf_op jit(solution)/shard_map/ppermute | solution.py:296
  43.7 12.0 %copy-start.2 = (bf16[1536,256]{1,0:T(8,128)(2,1)}, bf16[1536,256]{1,0:T(8,128)(2,1)S(1)}, u32[]{:S(2)}) copy-start(bf16[1536,256]{1,0:T(8,128)(2,1)S(1)} %collective-permute-done.sib_ref) | copy-start | bytes 2359300
  45.9 0.9 copy-start.4
  53.5 1.1 copy-start.5
  72.1 17.9 %copy-start.1 = (bf16[1536,256]{1,0:T(8,128)(2,1)S(1)}, bf16[1536,256]{1,0:T(8,128)(2,1)}, u32[]{:S(2)}) copy-start(bf16[1536,256]{1,0:T(8,128)(2,1)} %copy-done) | copy-start | bytes 2359300
  72.1 17.9 %copy-start.3 = (bf16[1536,256]{1,0:T(8,128)(2,1)S(1)}, bf16[1536,256]{1,0:T(8,128)(2,1)}, u32[]{:S(2)}) copy-start(bf16[1536,256]{1,0:T(8,128)(2,1)} %copy-done.2) | copy-start | bytes 2359300
  72.1 17.9 %copy-start.6 = (bf16[1536,256]{1,0:T(8,128)(2,1)S(1)}, bf16[1536,256]{1,0:T(8,128)(2,1)}, u32[]{:S(2)}) copy-start(bf16[1536,256]{1,0:T(8,128)(2,1)} %copy-done.4) | copy-start | bytes 2359300
  88.1 3.6 %copy-start.7 = (bf16[1536,256]{1,0:T(8,128)(2,1)}, bf16[1536,256]{1,0:T(8,128)(2,1)S(1)}, u32[]{:S(2)}) copy-start(bf16[1536,256]{1,0:T(8,128)(2,1)S(1)} %get-tuple-element.15.keep_ref) | copy-start | bytes 2359300
  88.1 3.6 %copy-start.9 = (bf16[1536,256]{1,0:T(8,128)(2,1)}, bf16[1536,256]{1,0:T(8,128)(2,1)S(1)}, u32[]{:S(2)}) copy-start(bf16[1536,256]{1,0:T(8,128)(2,1)S(1)} %get-tuple-element.17.pass_ref) | copy-start | bytes 2359300
  88.1 12.7 %collective-permute-start.3 = (bf16[2,1536,256]{2,1,0:T(8,128)(2,1)}, bf16[2,1536,256]{2,1,0:T(8,128)(2,1)S(1)}, u32[]{:S(2)}, u32[]{:S(2)}) collective-permute-start(bf16[2,1536,256]{2,1,0:T(8,128)(2,1)} %get-tuple-element.16), channel_id=1, source_target_pairs={{0,4},{4,0},{8,12},{12,8},{16,20},{20,16},{24,28},{28,24},{32,36},... | collective-permute-start | bytes 4718600 | tf_op jit(solution)/shard_map/ppermute | solution.py:320
  91.8 33.2 %all-to-all-start.2 = ((bf16[32,8,640]{2,1,0:T(8,128)(2,1)}), bf16[32,8,640]{2,1,0:T(8,128)(2,1)S(1)}, u32[]{:S(2)}, u32[]{:S(2)}) async-start(bf16[32,8,640]{2,1,0:T(8,128)(2,1)} %bitcast.8), calls=%async_computation.2 | async-start | bytes 655360 | tf_op jit(solution)/shard_map/all_to_all | solution.py:308
  100.8 1.1 copy-start.10
  102.0 23.0 %copy-start.11 = (s32[128,2]{0,1:T(2,128)S(1)}, s32[128,2]{0,1:T(2,128)}, u32[]{:S(2)}) copy-start(s32[128,2]{0,1:T(2,128)} %param.9) | copy-start | bytes 3076
  102.0 24.0 %copy-start.8 = (bf16[1536,256]{1,0:T(8,128)(2,1)S(1)}, bf16[1536,256]{1,0:T(8,128)(2,1)}, u32[]{:S(2)}) copy-start(bf16[1536,256]{1,0:T(8,128)(2,1)} %copy-done.7) | copy-start | bytes 2359300
  103.1 22.9 %collective-permute-start.4 = (bf16[1536,256]{1,0:T(8,128)(2,1)}, bf16[1536,256]{1,0:T(8,128)(2,1)}, u32[]{:S(2)}, u32[]{:S(2)}) collective-permute-start(bf16[1536,256]{1,0:T(8,128)(2,1)} %shard_map.116), channel_id=1, source_target_pairs={{0,8},{4,12},{8,0},{12,4},{16,24},{20,28},{24,16},{28,20},{32,40},... | collective-permute-start | bytes 2359304 | tf_op jit(solution)/shard_map/ppermute | solution.py:322

commit v3 on v2

--- a/solution.py
+++ b/solution.py
@@ -19,7 +19,14 @@
     groups = []
     for low in (0, 1):
         for core in (0, 1):
-            groups.append([z * 8 + x * 2 + core for x in (low, 3 - low) for z in range(planes)])
+            groups.append(
+                [
+                    z * 8 + x * 2 + core
+                    for near in range(planes // 2)
+                    for z in (near, near + planes // 2)
+                    for x in (low, 3 - low)
+                ]
+            )
     return groups
 
 
@@ -51,7 +58,10 @@
 def placement(experts, n_groups):
     toks = experts.shape[1]
     group = lax.shift_right_logical(experts[0:1, :], 2)
-    group = (group & 1) * (n_groups // 2) + lax.shift_right_logical(group, 1)
+    plane = lax.shift_right_logical(group, 1)
+    planes = n_groups // 2
+    plane = jnp.where(plane < planes // 2, 2 * plane, 2 * plane - planes + 1)
+    group = 2 * plane + (group & 1)
     member = iota((n_groups, toks), 0) == group
     onehot = jnp.where(member, 1.0, 0.0)
     earlier = jnp.where(iota((toks, toks), 0) < iota((toks, toks), 1), 1.0, 0.0).astype(BF)
@@ -102,39 +112,37 @@
     return jnp.broadcast_to(first, wide), jnp.broadcast_to(second, wide)
 
 
-def weights(w_refs, r, rows):
-    return w_refs[r][rows, :]
-
-
-def parts_kernel(arr_ref, own_ref, sib_ref, x_ref, xsib_ref, out_ref):
+def parts_kernel(arr_ref, own_ref, sib_ref, x_ref, xsib_hbm, out_ref, xsib_ref, acc_ref, sem):
+    fetch = pltpu.make_async_copy(xsib_hbm, xsib_ref, sem)
+    fetch.start()
     w_refs = (own_ref, sib_ref, x_ref, xsib_ref)
     hidden = own_ref.shape[1]
-    block = own_ref.shape[0] // 6 * 2
+    block = own_ref.shape[0] // 3
+    half = block // 2
     mine = lax.axis_index("ep") & (GROUP - 1)
     first, second = picks(arr_ref[:, 2 * block :].astype(F32), hidden)
-    rows = arr_ref[:, :block]
+
+    def dense(q, r):
+        if q < 2:
+            return dot(arr_ref[:, :block], w_refs[r][q * block : (q + 1) * block, :], 1, 0)
+        return dot(
+            arr_ref[:, block : block + half], w_refs[r][2 * block : 2 * block + half, :], 1, 1
+        ) + dot(arr_ref[:, block + half : 2 * block], w_refs[r][2 * block + half :, :], 1, 1)
+
     for q in range(3):
         p0 = jnp.zeros(first.shape, F32)
         p1 = p0
-        for r in ORDER:
-            if q < 2:
-                dense = dot(rows, weights(w_refs, r, slice(q * block, (q + 1) * block)), 1, 0)
-            else:
-                half = block // 2
-                dense = dot(
-                    arr_ref[:, block : block + half],
-                    weights(w_refs, r, slice(2 * block, 2 * block + half)),
-                    1,
-                    1,
-                ) + dot(
-                    arr_ref[:, block + half : 2 * block],
-                    weights(w_refs, r, slice(2 * block + half, 3 * block)),
-                    1,
-                    1,
-                )
-            expert = mine ^ r
-            p0 = jnp.where(first == expert, dense, p0)
-            p1 = jnp.where(second == expert, dense, p1)
+        for r in (0, 2, 1):
+            part = dense(q, r)
+            p0 = jnp.where(first == (mine ^ r), part, p0)
+            p1 = jnp.where(second == (mine ^ r), part, p1)
+        acc_ref[2 * q] = p0
+        acc_ref[2 * q + 1] = p1
+    fetch.wait()
+    for q in range(3):
+        part = dense(q, 3)
+        p0 = jnp.where(first == (mine ^ 3), part, acc_ref[2 * q])
+        p1 = jnp.where(second == (mine ^ 3), part, acc_ref[2 * q + 1])
         out_ref[:, q * hidden : (q + 1) * hidden] = p0.astype(BF)
         out_ref[:, (3 + q) * hidden : (4 + q) * hidden] = p1.astype(BF)
 
@@ -174,12 +182,12 @@
     out_ref[:, 6 * hidden :] = extra.astype(BF)
 
 
-def masks(arr_ref, hidden):
+def masks(arr_ref, hidden, experts=ORDER):
     mine = lax.axis_index("ep") & (GROUP - 1)
     meta = arr_ref[:, arr_ref.shape[1] - LANES :].astype(F32)
     first, second = picks(meta, hidden)
     out = {}
-    for r in ORDER:
+    for r in experts:
         expert = mine ^ r
         out[r] = tuple(jnp.where(p == expert, 1.0, 0.0).astype(BF) for p in (first, second))
     return out
@@ -192,60 +200,88 @@
     )
 
 
-def back_kernel(act_ref, arr_ref, own_ref, sib_ref, x_ref, xsib_ref, out_ref):
+def back_kernel(act_ref, arr_ref, own_ref, sib_ref, x_ref, xsib_hbm, out_ref, xsib_ref, sem):
+    hidden = own_ref.shape[1]
+    block = own_ref.shape[0] // 3
+    fetch = pltpu.make_async_copy(xsib_hbm.at[: 2 * block, :], xsib_ref, sem)
+    fetch.start()
     w_refs = (own_ref, sib_ref, x_ref, xsib_ref)
-    hidden = own_ref.shape[1]
-    block = own_ref.shape[0] // 6 * 2
     mask = masks(arr_ref, hidden)
     acc = jnp.zeros((act_ref.shape[0], block), F32)
     for r in ORDER:
+        if r == 3:
+            fetch.wait()
         for q in (1, 2):
-            w = weights(w_refs, r, slice((q - 1) * block, q * block))
+            w = w_refs[r][(q - 1) * block : q * block, :]
             acc = acc + dot(spread(act_ref, mask[r], q, hidden), w, 1, 1)
     out_ref[:, :block] = acc.astype(BF)
     out_ref[:, block:] = act_ref[:, 6 * hidden :]
 
 
-def stacked(block):
+def inner_parts(act_ref, arr_ref, mask, hidden):
+    rows = arr_ref[:, : (arr_ref.shape[1] - LANES) // 2]
+    return [dot(rows, spread(act_ref, mask, q, hidden), 0, 0) for q in (1, 2)]
+
+
+def outer_part(act_ref, arr_ref, mask, hidden):
+    block = (arr_ref.shape[1] - LANES) // 2
+    return dot(spread(act_ref, mask, 0, hidden), arr_ref[:, block : 2 * block], 0, 0)
+
+
+def inner_kernel(act_ref, arr_ref, send_ref, pass_ref):
+    hidden = send_ref.shape[1]
+    block = send_ref.shape[0] // 2
+    mask = masks(arr_ref, hidden, (2, 3))
+    for r, ref in ((3, send_ref), (2, pass_ref)):
+        gate, up = inner_parts(act_ref, arr_ref, mask[r], hidden)
+        ref[:block, :] = gate.astype(BF)
+        ref[block:, :] = up.astype(BF)
+
+
+def outer_kernel(act_ref, arr_ref, send_ref, pass_ref):
+    hidden = send_ref.shape[0]
+    mask = masks(arr_ref, hidden, (2, 3))
+    for r, ref in ((3, send_ref), (2, pass_ref)):
+        ref[...] = outer_part(act_ref, arr_ref, mask[r], hidden).astype(BF)
+
+
+def half_kernel(pass_ref, got_ref, out_ref):
+    out_ref[...] = (pass_ref[...].astype(F32) + got_ref[...].astype(F32)).astype(BF)
+
+
+def sibling_kernel(act_ref, arr_ref, out_ref):
+    hidden = out_ref.shape[1]
+    block = out_ref.shape[0] // 3
     half = block // 2
-    return (
-        slice(0, block),
-        slice(block, 2 * block),
-        slice(2 * block, 2 * block + half),
-        slice(2 * block + half, 3 * block),
-    )
-
-
-def grads_kernel(act_ref, arr_ref, send_ref, pass_ref, keep_ref):
-    hidden = send_ref.shape[2]
-    block = send_ref.shape[1] // 3
-    g, u, d0, d1 = stacked(block)
-    mask = masks(arr_ref, hidden)
-    rows = arr_ref[:, :block]
-    cots = arr_ref[:, block : 2 * block]
-    for r, ref in ((1, send_ref.at[0]), (3, send_ref.at[1]), (2, pass_ref), (0, keep_ref)):
-        ref[g, :] = dot(rows, spread(act_ref, mask[r], 1, hidden), 0, 0).astype(BF)
-        ref[u, :] = dot(rows, spread(act_ref, mask[r], 2, hidden), 0, 0).astype(BF)
-        down = dot(spread(act_ref, mask[r], 0, hidden), cots, 0, 0).astype(BF)
-        ref[d0, :] = down[:, : block // 2]
-        ref[d1, :] = down[:, block // 2 :]
-
-
-def half_kernel(pass_ref, got_ref, out_ref):
-    out_ref[...] = (pass_ref[...].astype(F32) + got_ref[1].astype(F32)).astype(BF)
-
-
-def total_kernel(keep_ref, got_ref, last_ref, gate_ref, up_ref, down_ref):
-    block = gate_ref.shape[0]
-    g, u, d0, d1 = stacked(block)
-
-    def total(at):
-        return keep_ref[at, :].astype(F32) + got_ref[0, at, :].astype(F32) + last_ref[at, :].astype(F32)
-
-    gate_ref[...] = total(g)
-    up_ref[...] = total(u)
-    down_ref[:, : block // 2] = total(d0)
-    down_ref[:, block // 2 :] = total(d1)
+    mask = masks(arr_ref, hidden, (1,))[1]
+    gate, up = inner_parts(act_ref, arr_ref, mask, hidden)
+    down = outer_part(act_ref, arr_ref, mask, hidden).astype(BF)
+    out_ref[:block, :] = gate.astype(BF)
+    out_ref[block : 2 * block, :] = up.astype(BF)
+    out_ref[2 * block : 2 * block + half, :] = down[:, :half]
+    out_ref[2 * block + half :, :] = down[:, half:]
+
+
+def base_kernel(act_ref, arr_ref, got_ref, inner_ref, outer_ref):
+    hidden = inner_ref.shape[1]
+    block = inner_ref.shape[0] // 2
+    half = block // 2
+    mask = masks(arr_ref, hidden, (0,))[0]
+    gate, up = inner_parts(act_ref, arr_ref, mask, hidden)
+    down = outer_part(act_ref, arr_ref, mask, hidden)
+    inner_ref[:block, :] = (gate + got_ref[:block, :].astype(F32)).astype(BF)
+    inner_ref[block:, :] = (up + got_ref[block : 2 * block, :].astype(F32)).astype(BF)
+    left = down[:, :half] + got_ref[2 * block : 2 * block + half, :].astype(F32)
+    right = down[:, half:] + got_ref[2 * block + half :, :].astype(F32)
+    outer_ref[:, :half] = left.astype(BF)
+    outer_ref[:, half:] = right.astype(BF)
+
+
+def total_kernel(base_ref, last_ref, *out_refs):
+    rows = out_refs[0].shape[0]
+    for i, out_ref in enumerate(out_refs):
+        at = slice(i * rows, (i + 1) * rows)
+        out_ref[...] = base_ref[at, :].astype(F32) + last_ref[at, :].astype(F32)
 
 
 def final_kernel(ret_ref, exp_ref, tok_ref, comb_ref):
@@ -295,16 +331,36 @@
     sibling = lax.ppermute(own, "ep", partner(peers, 1))
     across = lax.ppermute(other, "ep", partner(peers, 1))
     w_all = tuple(
-        pltpu.with_memory_space_constraint(w, pltpu.VMEM) for w in (own, sibling, other, across)
-    )
-    parts = call(parts_kernel, shape((slots, 6 * hidden), BF), arrived, *w_all)
+        pltpu.with_memory_space_constraint(w, space)
+        for w, space in zip((own, sibling, other, across), (pltpu.VMEM,) * 3 + (pltpu.HBM,))
+    )
+    parts = call(
+        parts_kernel,
+        shape((slots, 6 * hidden), BF),
+        arrived,
+        *w_all,
+        in_specs=[pl.BlockSpec(memory_space=pltpu.HBM if i == 4 else pltpu.VMEM) for i in range(5)],
+        scratch_shapes=[
+            pltpu.VMEM((3 * block, hidden), BF),
+            pltpu.VMEM((6, slots, hidden), F32),
+            pltpu.SemaphoreType.DMA,
+        ],
+    )
     pieces = lax.all_to_all(
         parts.reshape(widths, share, -1), "tp", split_axis=0, concat_axis=0, tiled=True
     )
     acts = call(act_kernel, shape((share, 6 * hidden + LANES), BF), pieces, arrived)
     acts = lax.all_gather(acts, "tp", axis=0, tiled=True)
     acts = pltpu.with_memory_space_constraint(acts, pltpu.VMEM)
-    back = call(back_kernel, shape((slots, block + LANES), BF), acts, arrived, *w_all)
+    back = call(
+        back_kernel,
+        shape((slots, block + LANES), BF),
+        acts,
+        arrived,
+        *w_all,
+        in_specs=[pl.BlockSpec(memory_space=pltpu.HBM if i == 5 else pltpu.VMEM) for i in range(6)],
+        scratch_shapes=[pltpu.VMEM((2 * block, hidden), BF), pltpu.SemaphoreType.DMA],
+    )
     returned = lax.all_to_all(
         back.reshape(n_groups, CAP, -1),
         "ep",
@@ -313,20 +369,26 @@
         tiled=True,
         axis_index_groups=groups,
     ).reshape(slots, -1)
-    stack = (3 * block, hidden)
-    send, through, keep = call(
-        grads_kernel, (shape((2, *stack), BF), shape(stack, BF), shape(stack, BF)), acts, arrived
-    )
+    pairs = []
+    for kernel, inputs, dims in (
+        (inner_kernel, (acts, arrived), (2 * block, hidden)),
+        (outer_kernel, (acts, arrived), (hidden, block)),
+    ):
+        send, through = call(kernel, (shape(dims, BF), shape(dims, BF)), *inputs)
+        got = lax.ppermute(send, "ep", partner(peers, 1))
+        pair = call(half_kernel, shape(dims, BF), through, got)
+        pairs.append(lax.ppermute(pair, "ep", partner(peers, 2)))
+    send = call(sibling_kernel, shape((3 * block, hidden), BF), acts, arrived)
     got = lax.ppermute(send, "ep", partner(peers, 1))
-    pair = call(half_kernel, shape(stack, BF), through, got)
-    last = lax.ppermute(pair, "ep", partner(peers, 2))
-    gate_grad, up_grad, down_grad = call(
-        total_kernel,
-        (shape((block, hidden), F32), shape((block, hidden), F32), shape((hidden, block), F32)),
-        keep,
+    base = call(
+        base_kernel,
+        (shape((2 * block, hidden), BF), shape((hidden, block), BF)),
+        acts,
+        arrived,
         got,
-        last,
-    )
+    )
+    gate_grad, up_grad = call(total_kernel, (shape((block, hidden), F32),) * 2, base[0], pairs[0])
+    (down_grad,) = call(total_kernel, (shape((hidden, block), F32),), base[1], pairs[1])
     grad_tokens, comb = call(
         final_kernel, (shape((toks, block), BF), shape((2, toks), F32)), returned, experts.T
     )

time: 130 us -> 130 us (level)
  starting transfers between devices: 36.5 us -> 47.4 us
  waiting for transfers between devices: 45.6 us -> 40.3 us
  local copies, waits for them, and re-layouts: 3.23 us -> 0.05 us
  blocking collectives: 30 us -> 28.5 us
    all_to_all x1, waiting for transfers between devices: 19.9 us -> 0.01 us  [body(): lax.all_to_all(back.reshape(n_groups, CAP, -1), 'ep', split_axis=0, conca...]
    ppermute x1 -> x2, waiting for transfers between devices: 0.01 us -> 15.3 us  [body(): pairs.append(lax.ppermute(pair, 'ep', partner(peers, 2)))]
    ppermute x1 -> x3, starting transfers between devices: 1.91 us -> 6.25 us  [body(): got = lax.ppermute(send, 'ep', partner(peers, 1))]
    ppermute x1 -> x2, starting transfers between devices: 1.91 us -> 5.84 us  [body(): pairs.append(lax.ppermute(pair, 'ep', partner(peers, 2)))]
    unnamed x30 -> x12, local copies, waits for them, and re-layouts: 3.21 us -> 0.03 us
    all_to_all x1, starting transfers between devices: 9.04 us -> 11.5 us  [body(): lax.all_to_all(back.reshape(n_groups, CAP, -1), 'ep', split_axis=0, conca...]
    pallas_call x8 -> x13, Pallas kernels: 12 us -> 12 us  [call(): pl.pallas_call(kernel, out_shape=outs, compiler_params=pltpu.CompilerPara...]
  transfers between devices with their start and end apart: 7 -> 10, of which waited for: 4 -> 4; matrix products, arithmetic and copies ran while one was open for 0% -> 0% of each run, Pallas kernels for 3% -> 3%
where the time goes in v3:
time: 130 us; the launch traced here: 129 us
  starting transfers between devices  47.4 us (36%)
  waiting for transfers between devices  40.3 us (31%)
  blocking collectives  28.5 us (22%)
  Pallas kernels  12 us (9%)
    all_to_all x1, starting transfers between devices, body(): lax.all_to_all(payload.reshape(n_groups, CAP, -1), 'ep', split_axis=0, co...  18.1 us
    ppermute x1, waiting for transfers between devices, body(): other = lax.ppermute(own, 'ep', partner(peers, 2))  16.8 us
    ppermute x2, waiting for transfers between devices, body(): pairs.append(lax.ppermute(pair, 'ep', partner(peers, 2)))  15.3 us
    all_to_all x1, blocking collectives, body(): lax.all_to_all(parts.reshape(widths, share, -1), 'tp', split_axis=0, conc...  14.9 us
    all_gather x1, blocking collectives, body(): acts = lax.all_gather(acts, 'tp', axis=0, tiled=True)  13.6 us
    pallas_call x13, Pallas kernels, call(): pl.pallas_call(kernel, out_shape=outs, compiler_params=pltpu.CompilerPara...  12 us
    all_to_all x1, starting transfers between devices, body(): lax.all_to_all(back.reshape(n_groups, CAP, -1), 'ep', split_axis=0, conca...  11.5 us
    ppermute x3, starting transfers between devices, body(): got = lax.ppermute(send, 'ep', partner(peers, 1))  6.25 us
  transfers between devices with their start and end apart: 10, of which 4 were waited for; matrix products, arithmetic and copies ran while one was open for 0% of the time, Pallas kernels for 3%

profile of v3, /device:TPU:6, one launch (start us, length us, event | category | flops | bytes accessed | tf_op | source)
XLA Modules:
  0.0 129.2 jit_solution(16733935426339371954)
XLA Ops:
  0.6 2.3 %shard_map.110 = bf16[256,1152]{1,0:T(8,128)(2,1)} custom-call(bf16[128,512]{1,0:T(8,128)(2,1)} %tok_hbm.1, bf16[128,512]{1,0:T(8,128)(2,1)} %cot_hbm.1, s32[2,128]{1,0:T(2,128)} %bitcast.23, f32[2,128]{1,0:T(2,128)} %bitcast.29), custom_call_target="tpu_custom_call" | custom-call | tf_op jit(solution)/shard_map/pallas_call | solution.py:46
  3.0 0.0 copy-start.4
  3.0 0.0 copy-start.5
  3.0 18.1 %all-to-all-start = ((bf16[32,8,1152]{2,1,0:T(8,128)(2,1)}), bf16[32,8,1152]{2,1,0:T(8,128)(2,1)S(1)}, u32[]{:S(2)}, u32[]{:S(2)}) async-start(bf16[32,8,1152]{2,1,0:T(8,128)(2,1)} %bitcast.2), calls=%async_computation | async-start | bytes 1179648 | tf_op jit(solution)/shard_map/all_to_all | solution.py:320
  21.1 0.1 pad_maximum_fusion.own_ref
  21.2 1.9 %collective-permute-start.1 = (bf16[1536,256]{1,0:T(8,128)(2,1)S(1)}, bf16[1536,256]{1,0:T(8,128)(2,1)S(1)}, u32[]{:S(2)}, u32[]{:S(2)}) collective-permute-start(bf16[1536,256]{1,0:T(8,128)(2,1)S(1)} %pad_maximum_fusion.own_ref), channel_id=1, source_target_pairs={{0,8},{4,12},{8,0},{12,4},{16,24},{20,28},{24,16},{28,20},{32,40},... | collective-permute-start | bytes 2359304 | tf_op jit(solution)/shard_map/ppermute | solution.py:330
  23.1 1.9 %collective-permute-start = (bf16[1536,256]{1,0:T(8,128)(2,1)S(1)}, bf16[1536,256]{1,0:T(8,128)(2,1)S(1)}, u32[]{:S(2)}, u32[]{:S(2)}) collective-permute-start(bf16[1536,256]{1,0:T(8,128)(2,1)S(1)} %pad_maximum_fusion.own_ref), channel_id=1, source_target_pairs={{0,4},{4,0},{8,12},{12,8},{16,20},{20,16},{24,28},{28,24},{32,36},... | collective-permute-start | bytes 2359304 | tf_op jit(solution)/shard_map/ppermute | solution.py:331
  25.0 16.8 %collective-permute-done.1.x_ref = bf16[1536,256]{1,0:T(8,128)(2,1)S(1)} collective-permute-done((bf16[1536,256]{1,0:T(8,128)(2,1)S(1)}, bf16[1536,256]{1,0:T(8,128)(2,1)S(1)}, u32[]{:S(2)}, u32[]{:S(2)}) %collective-permute-start.1) | collective-permute-done | bytes 786464 | tf_op jit(solution)/shard_map/ppermute | solution.py:330
  41.8 1.9 %collective-permute-start.2 = (bf16[1536,256]{1,0:T(8,128)(2,1)S(1)}, bf16[1536,256]{1,0:T(8,128)(2,1)}, u32[]{:S(2)}, u32[]{:S(2)}) collective-permute-start(bf16[1536,256]{1,0:T(8,128)(2,1)S(1)} %collective-permute-done.1.x_ref), channel_id=1, source_target_pairs={{0,4},{4,0},{8,12},{12,8},{16,20},{20,16},{24,28},{28,24},{32,36},... | collective-permute-start | bytes 2359304 | tf_op jit(solution)/shard_map/ppermute | solution.py:332
  43.7 2.4 %collective-permute-done.2.xsib_hbm = bf16[1536,256]{1,0:T(8,128)(2,1)} collective-permute-done((bf16[1536,256]{1,0:T(8,128)(2,1)S(1)}, bf16[1536,256]{1,0:T(8,128)(2,1)}, u32[]{:S(2)}, u32[]{:S(2)}) %collective-permute-start.2) | collective-permute-done | bytes 786464 | tf_op jit(solution)/shard_map/ppermute | solution.py:332
  46.1 5.9 %all-to-all-done = bf16[32,8,1152]{2,1,0:T(8,128)(2,1)S(1)} async-done(((bf16[32,8,1152]{2,1,0:T(8,128)(2,1)}), bf16[32,8,1152]{2,1,0:T(8,128)(2,1)S(1)}, u32[]{:S(2)}, u32[]{:S(2)}) %all-to-all-start) | async-done | bytes 589856 | tf_op jit(solution)/shard_map/all_to_all | solution.py:320
  52.0 1.6 %shard_map.111 = bf16[256,1536]{1,0:T(8,128)(2,1)S(1)} custom-call(bf16[256,1152]{1,0:T(8,128)(2,1)S(1)} %bitcast.14, bf16[1536,256]{1,0:T(8,128)(2,1)S(1)} %pad_maximum_fusion.own_ref, bf16[1536,256]{1,0:T(8,128)(2,1)S(1)} %collective-permute-done.sib_ref, bf16[1536,256]{1,0:T(8,128)(2,1)S(1)} %collective-permute-done.1.x_ref, ...), custom_call_target="tpu_custom_call" | custom-call | tf_op jit(solution)/shard_map/pallas_call | solution.py:46
  53.7 14.9 %all_to_all.15.part_ref = bf16[4,64,1536]{2,1,0:T(8,128)(2,1)S(1)} all-to-all(bf16[4,64,1536]{2,1,0:T(8,128)(2,1)S(1)} %bitcast.21), channel_id=1, replica_groups=mesh['ep'=128,'tp'=4] {'tp'}, dimensions={0} | all-to-all | bytes 1572864 | tf_op jit(solution)/shard_map/all_to_all | solution.py:349
  68.6 0.3 shard_map.112
  68.8 13.6 %all_gather.3.act_ref = bf16[256,1664]{1,0:T(8,128)(2,1)S(1)} all-gather(bf16[64,1664]{1,0:T(8,128)(2,1)S(1)} %shard_map.112), channel_id=1, replica_groups=mesh['ep'=128,'tp'=4] {'tp'}, dimensions={0}, use_global_device_ids=true | all-gather | bytes 1064960 | tf_op jit(solution)/shard_map/all_gather | solution.py:353
  82.4 2.2 %shard_map.113 = bf16[256,640]{1,0:T(8,128)(2,1)} custom-call(bf16[256,1664]{1,0:T(8,128)(2,1)S(1)} %all_gather.3.act_ref, bf16[256,1152]{1,0:T(8,128)(2,1)S(1)} %bitcast.16, bf16[1536,256]{1,0:T(8,128)(2,1)S(1)} %pad_maximum_fusion.own_ref, bf16[1536,256]{1,0:T(8,128)(2,1)S(1)} %copy-done.1, bf16[1536,256]{1,0:T(8,128)(2,1)S(1)} %collective-permute-done.1.x_ref, ...), custom_call_target="tpu_custom_call" | custom-call | tf_op jit(solution)/shard_map/pallas_call | solution.py:46
  84.7 11.5 %all-to-all-start.2 = ((bf16[32,8,640]{2,1,0:T(8,128)(2,1)}), bf16[32,8,640]{2,1,0:T(8,128)(2,1)S(1)}, u32[]{:S(2)}, u32[]{:S(2)}) async-start(bf16[32,8,640]{2,1,0:T(8,128)(2,1)} %bitcast.8), calls=%async_computation.2 | async-start | bytes 655360 | tf_op jit(solution)/shard_map/all_to_all | solution.py:364
  96.2 0.7 shard_map.117
  96.8 1.9 %collective-permute-start.4 = (bf16[1024,256]{1,0:T(8,128)(2,1)S(1)}, bf16[1024,256]{1,0:T(8,128)(2,1)S(1)}, u32[]{:S(2)}, u32[]{:S(2)}) collective-permute-start(bf16[1024,256]{1,0:T(8,128)(2,1)S(1)} %get-tuple-element.19), channel_id=1, source_target_pairs={{0,4},{4,0},{8,12},{12,8},{16,20},{20,16},{24,28},{28,24},{32,36},... | collective-permute-start | bytes 1572872 | tf_op jit(solution)/shard_map/ppermute | solution.py:378
  98.8 0.6 shard_map.115
  99.4 2.4 %collective-permute-start.3 = (bf16[1536,256]{1,0:T(8,128)(2,1)S(1)}, bf16[1536,256]{1,0:T(8,128)(2,1)S(1)}, u32[]{:S(2)}, u32[]{:S(2)}) collective-permute-start(bf16[1536,256]{1,0:T(8,128)(2,1)S(1)} %shard_map.115), channel_id=1, source_target_pairs={{0,4},{4,0},{8,12},{12,8},{16,20},{20,16},{24,28},{28,24},{32,36},... | collective-permute-start | bytes 2359304 | tf_op jit(solution)/shard_map/ppermute | solution.py:382
  101.8 0.6 shard_map.120
  102.3 1.9 %collective-permute-start.6 = (bf16[256,512]{1,0:T(8,128)(2,1)S(1)}, bf16[256,512]{1,0:T(8,128)(2,1)S(1)}, u32[]{:S(2)}, u32[]{:S(2)}) collective-permute-start(bf16[256,512]{1,0:T(8,128)(2,1)S(1)} %get-tuple-element.24), channel_id=1, source_target_pairs={{0,4},{4,0},{8,12},{12,8},{16,20},{20,16},{24,28},{28,24},{32,36},... | collective-permute-start | bytes 786440 | tf_op jit(solution)/shard_map/ppermute | solution.py:378
  104.3 0.1 shard_map.118
  104.4 1.9 %collective-permute-start.5 = (bf16[1024,256]{1,0:T(8,128)(2,1)S(1)}, bf16[1024,256]{1,0:T(8,128)(2,1)S(1)}, u32[]{:S(2)}, u32[]{:S(2)}) collective-permute-start(bf16[1024,256]{1,0:T(8,128)(2,1)S(1)} %shard_map.118), channel_id=1, source_target_pairs={{0,8},{4,12},{8,0},{12,4},{16,24},{20,28},{24,16},{28,20},{32,40},... | collective-permute-start | bytes 1572872 | tf_op jit(solution)/shard_map/ppermute | solution.py:380
  106.4 0.1 shard_map.121
  106.4 3.9 %collective-permute-start.7 = (bf16[256,512]{1,0:T(8,128)(2,1)S(1)}, bf16[256,512]{1,0:T(8,128)(2,1)S(1)}, u32[]{:S(2)}, u32[]{:S(2)}) collective-permute-start(bf16[256,512]{1,0:T(8,128)(2,1)S(1)} %shard_map.121), channel_id=1, source_target_pairs={{0,8},{4,12},{8,0},{12,4},{16,24},{20,28},{24,16},{28,20},{32,40},... | collective-permute-start | bytes 786440 | tf_op jit(solution)/shard_map/ppermute | solution.py:380
  110.4 0.6 shard_map.116
  111.0 15.3 %collective-permute-done.7.last_ref = bf16[256,512]{1,0:T(8,128)(2,1)S(1)} collective-permute-done((bf16[256,512]{1,0:T(8,128)(2,1)S(1)}, bf16[256,512]{1,0:T(8,128)(2,1)S(1)}, u32[]{:S(2)}, u32[]{:S(2)}) %collective-permute-start.7) | collective-permute-done | bytes 262176 | tf_op jit(solution)/shard_map/ppermute | solution.py:380
  126.3 0.8 shard_map.122
  127.1 1.0 shard_map.119
  128.1 1.0 shard_map.114
  (17 shorter events, 0.1 us)
Async XLA Ops:
  0.6 20.4 %copy-start.3 = (bf16[1,256,512]{2,1,0:T(8,128)(2,1)S(1)}, bf16[1,256,512]{2,1,0:T(8,128)(2,1)}, u32[]{:S(2)}) copy-start(bf16[1,256,512]{2,1,0:T(8,128)(2,1)} %param.13) | copy-start | bytes 786436
  3.0 18.1 %copy-start.4 = (bf16[1,512,256]{2,1,0:T(8,128)(2,1)S(1)}, bf16[1,512,256]{2,1,0:T(8,128)(2,1)}, u32[]{:S(2)}) copy-start(bf16[1,512,256]{2,1,0:T(8,128)(2,1)} %param.12) | copy-start | bytes 786436
  3.0 18.1 %copy-start.5 = (bf16[1,512,256]{2,1,0:T(8,128)(2,1)S(1)}, bf16[1,512,256]{2,1,0:T(8,128)(2,1)}, u32[]{:S(2)}) copy-start(bf16[1,512,256]{2,1,0:T(8,128)(2,1)} %param.11) | copy-start | bytes 786436
  3.0 49.0 %all-to-all-start = ((bf16[32,8,1152]{2,1,0:T(8,128)(2,1)}), bf16[32,8,1152]{2,1,0:T(8,128)(2,1)S(1)}, u32[]{:S(2)}, u32[]{:S(2)}) async-start(bf16[32,8,1152]{2,1,0:T(8,128)(2,1)} %bitcast.2), calls=%async_computation | async-start | bytes 1179648 | tf_op jit(solution)/shard_map/all_to_all | solution.py:320
  21.2 20.6 %collective-permute-start.1 = (bf16[1536,256]{1,0:T(8,128)(2,1)S(1)}, bf16[1536,256]{1,0:T(8,128)(2,1)S(1)}, u32[]{:S(2)}, u32[]{:S(2)}) collective-permute-start(bf16[1536,256]{1,0:T(8,128)(2,1)S(1)} %pad_maximum_fusion.own_ref), channel_id=1, source_target_pairs={{0,8},{4,12},{8,0},{12,4},{16,24},{20,28},{24,16},{28,20},{32,40},... | collective-permute-start | bytes 2359304 | tf_op jit(solution)/shard_map/ppermute | solution.py:330
  23.1 20.6 %collective-permute-start = (bf16[1536,256]{1,0:T(8,128)(2,1)S(1)}, bf16[1536,256]{1,0:T(8,128)(2,1)S(1)}, u32[]{:S(2)}, u32[]{:S(2)}) collective-permute-start(bf16[1536,256]{1,0:T(8,128)(2,1)S(1)} %pad_maximum_fusion.own_ref), channel_id=1, source_target_pairs={{0,4},{4,0},{8,12},{12,8},{16,20},{20,16},{24,28},{28,24},{32,36},... | collective-permute-start | bytes 2359304 | tf_op jit(solution)/shard_map/ppermute | solution.py:331
  41.8 4.3 %collective-permute-start.2 = (bf16[1536,256]{1,0:T(8,128)(2,1)S(1)}, bf16[1536,256]{1,0:T(8,128)(2,1)}, u32[]{:S(2)}, u32[]{:S(2)}) collective-permute-start(bf16[1536,256]{1,0:T(8,128)(2,1)S(1)} %collective-permute-done.1.x_ref), channel_id=1, source_target_pairs={{0,4},{4,0},{8,12},{12,8},{16,20},{20,16},{24,28},{28,24},{32,36},... | collective-permute-start | bytes 2359304 | tf_op jit(solution)/shard_map/ppermute | solution.py:332
  43.7 9.9 %copy-start = (bf16[1536,256]{1,0:T(8,128)(2,1)}, bf16[1536,256]{1,0:T(8,128)(2,1)S(1)}, u32[]{:S(2)}) copy-start(bf16[1536,256]{1,0:T(8,128)(2,1)S(1)} %collective-permute-done.sib_ref) | copy-start | bytes 2359300
  68.8 13.6 %copy-start.1 = (bf16[1536,256]{1,0:T(8,128)(2,1)S(1)}, bf16[1536,256]{1,0:T(8,128)(2,1)}, u32[]{:S(2)}) copy-start(bf16[1536,256]{1,0:T(8,128)(2,1)} %copy-done) | copy-start | bytes 2359300
  84.7 43.5 %all-to-all-start.2 = ((bf16[32,8,640]{2,1,0:T(8,128)(2,1)}), bf16[32,8,640]{2,1,0:T(8,128)(2,1)S(1)}, u32[]{:S(2)}, u32[]{:S(2)}) async-start(bf16[32,8,640]{2,1,0:T(8,128)(2,1)} %bitcast.8), calls=%async_computation.2 | async-start | bytes 655360 | tf_op jit(solution)/shard_map/all_to_all | solution.py:364
  96.8 7.4 %collective-permute-start.4 = (bf16[1024,256]{1,0:T(8,128)(2,1)S(1)}, bf16[1024,256]{1,0:T(8,128)(2,1)S(1)}, u32[]{:S(2)}, u32[]{:S(2)}) collective-permute-start(bf16[1024,256]{1,0:T(8,128)(2,1)S(1)} %get-tuple-element.19), channel_id=1, source_target_pairs={{0,4},{4,0},{8,12},{12,8},{16,20},{20,16},{24,28},{28,24},{32,36},... | collective-permute-start | bytes 1572872 | tf_op jit(solution)/shard_map/ppermute | solution.py:378
  99.4 11.0 %collective-permute-start.3 = (bf16[1536,256]{1,0:T(8,128)(2,1)S(1)}, bf16[1536,256]{1,0:T(8,128)(2,1)S(1)}, u32[]{:S(2)}, u32[]{:S(2)}) collective-permute-start(bf16[1536,256]{1,0:T(8,128)(2,1)S(1)} %shard_map.115), channel_id=1, source_target_pairs={{0,4},{4,0},{8,12},{12,8},{16,20},{20,16},{24,28},{28,24},{32,36},... | collective-permute-start | bytes 2359304 | tf_op jit(solution)/shard_map/ppermute | solution.py:382
  102.3 4.0 %collective-permute-start.6 = (bf16[256,512]{1,0:T(8,128)(2,1)S(1)}, bf16[256,512]{1,0:T(8,128)(2,1)S(1)}, u32[]{:S(2)}, u32[]{:S(2)}) collective-permute-start(bf16[256,512]{1,0:T(8,128)(2,1)S(1)} %get-tuple-element.24), channel_id=1, source_target_pairs={{0,4},{4,0},{8,12},{12,8},{16,20},{20,16},{24,28},{28,24},{32,36},... | collective-permute-start | bytes 786440 | tf_op jit(solution)/shard_map/ppermute | solution.py:378
  104.4 22.7 %collective-permute-start.5 = (bf16[1024,256]{1,0:T(8,128)(2,1)S(1)}, bf16[1024,256]{1,0:T(8,128)(2,1)S(1)}, u32[]{:S(2)}, u32[]{:S(2)}) collective-permute-start(bf16[1024,256]{1,0:T(8,128)(2,1)S(1)} %shard_map.118), channel_id=1, source_target_pairs={{0,8},{4,12},{8,0},{12,4},{16,24},{20,28},{24,16},{28,20},{32,40},... | collective-permute-start | bytes 1572872 | tf_op jit(solution)/shard_map/ppermute | solution.py:380
  106.4 19.8 %collective-permute-start.7 = (bf16[256,512]{1,0:T(8,128)(2,1)S(1)}, bf16[256,512]{1,0:T(8,128)(2,1)S(1)}, u32[]{:S(2)}, u32[]{:S(2)}) collective-permute-start(bf16[256,512]{1,0:T(8,128)(2,1)S(1)} %shard_map.121), channel_id=1, source_target_pairs={{0,8},{4,12},{8,0},{12,4},{16,24},{20,28},{24,16},{28,20},{32,40},... | collective-permute-start | bytes 786440 | tf_op jit(solution)/shard_map/ppermute | solution.py:380
  126.2 1.9 %copy-start.2 = (s32[128,2]{0,1:T(2,128)S(1)}, s32[128,2]{0,1:T(2,128)}, u32[]{:S(2)}) copy-start(s32[128,2]{0,1:T(2,128)} %param.9) | copy-start | bytes 3076

commit v4 on v3

--- a/solution.py
+++ b/solution.py
@@ -22,8 +22,8 @@
             groups.append(
                 [
                     z * 8 + x * 2 + core
-                    for near in range(planes // 2)
-                    for z in (near, near + planes // 2)
+                    for near in range(planes // 4)
+                    for z in (near + planes // 4 * q for q in (0, 2, 1, 3))
                     for x in (low, 3 - low)
                 ]
             )
@@ -60,7 +60,9 @@
     group = lax.shift_right_logical(experts[0:1, :], 2)
     plane = lax.shift_right_logical(group, 1)
     planes = n_groups // 2
-    plane = jnp.where(plane < planes // 2, 2 * plane, 2 * plane - planes + 1)
+    quarter = plane // (planes // 4)
+    middle = (quarter == 1) | (quarter == 2)
+    plane = plane % (planes // 4) * 4 + jnp.where(middle, 3 - quarter, quarter)
     group = 2 * plane + (group & 1)
     member = iota((n_groups, toks), 0) == group
     onehot = jnp.where(member, 1.0, 0.0)
@@ -71,31 +73,46 @@
     return jnp.where(iota((n_groups * CAP, toks), 0) == slot, 1.0, 0.0).astype(BF)
 
 
-def send_kernel(tok_hbm, cot_hbm, exp_hbm, comb_hbm, out_ref, tok_ref, cot_ref, exp_ref, comb_ref, sems):
+def send_kernel(
+    tok_hbm, cot_hbm, exp_hbm, comb_hbm, out_hbm, tok_ref, cot_ref, exp_ref, comb_ref, out_ref, sems
+):
     copies = [
         pltpu.make_async_copy(src, dst, sems.at[i])
         for i, (src, dst) in enumerate(
-            ((exp_hbm, exp_ref), (comb_hbm, comb_ref), (tok_hbm, tok_ref), (cot_hbm, cot_ref))
+            ((exp_hbm, exp_ref), (tok_hbm, tok_ref), (cot_hbm, cot_ref), (comb_hbm, comb_ref))
         )
     ]
     for copy in copies:
         copy.start()
-    for copy in copies:
-        copy.wait()
-    block = tok_ref.shape[1]
-    toks = tok_ref.shape[0]
+    toks, block = tok_ref.shape
     n_groups = out_ref.shape[0] // CAP
+    copies[0].wait()
     experts = exp_ref[...]
     place = placement(experts, n_groups)
     local = experts & (GROUP - 1)
+    row = iota((LANES, toks), 0)
+
+    def written(first, last, i):
+        copy = pltpu.make_async_copy(
+            out_ref.at[:, first:last], out_hbm.at[:, first:last], sems.at[len(copies) + i]
+        )
+        copy.start()
+        return copy
+
+    copies[1].wait()
+    out_ref[:, :block] = dot(place, tok_ref[...], 1, 0).astype(BF)
+    rows_out = written(0, block, 0)
+    copies[2].wait()
+    copies[3].wait()
     weight = comb_ref[...].astype(BF).astype(F32)
-    row = iota((LANES, toks), 0)
     meta = jnp.where(row == local[0:1, :], weight[0:1, :], 0.0) + jnp.where(
         row == local[1:2, :], weight[1:2, :], 0.0
     )
-    out_ref[:, :block] = dot(place, tok_ref[...], 1, 0).astype(BF)
     out_ref[:, block : 2 * block] = dot(place, cot_ref[...], 1, 0).astype(BF)
     out_ref[:, 2 * block :] = dot(place, meta.astype(BF), 1, 1).astype(BF)
+    rest_out = written(block, 2 * block + LANES, 1)
+    rows_out.wait()
+    rest_out.wait()
 
 
 def chosen(meta):
@@ -152,6 +169,11 @@
     hidden = part_ref.shape[2] // 6
     meta_at = arr_ref.shape[1] - LANES
     me = lax.axis_index("tp")
+
+    def put(at, value):
+        for copy in range(out_ref.shape[0]):
+            out_ref[copy, :, at : at + value.shape[1]] = value
+
     meta = arr_ref[pl.ds(pl.multiple_of(me * share, share), share), meta_at:].astype(F32)
     first, second = chosen(meta)
     lane = iota((share, LANES), 1)
@@ -171,15 +193,13 @@
         hid = silu * up_pre
         gh = weight * grad_scaled
         at = 3 * k * hidden
-        out_ref[:, at : at + hidden] = (weight * hid).astype(BF)
-        out_ref[:, at + hidden : at + 2 * hidden] = (
-            gh * up_pre * sig * (1.0 + gate_pre * (1.0 - sig))
-        ).astype(BF)
-        out_ref[:, at + 2 * hidden : at + 3 * hidden] = (gh * silu).astype(BF)
+        put(at, (weight * hid).astype(BF))
+        put(at + hidden, (gh * up_pre * sig * (1.0 + gate_pre * (1.0 - sig))).astype(BF))
+        put(at + 2 * hidden, (gh * silu).astype(BF))
         comb = jnp.sum(hid * grad_scaled, axis=1, keepdims=True)
         high = comb.astype(BF).astype(F32)
         extra = jnp.where(lane == 2 * k, high, jnp.where(lane == 2 * k + 1, comb - high, extra))
-    out_ref[:, 6 * hidden :] = extra.astype(BF)
+    put(6 * hidden, extra.astype(BF))
 
 
 def masks(arr_ref, hidden, experts=ORDER):
@@ -314,8 +334,9 @@
         shape((slots, 2 * block + LANES), BF),
         *(pltpu.with_memory_space_constraint(a, pltpu.HBM) for a in sources),
         in_specs=[pl.BlockSpec(memory_space=pltpu.HBM)] * 4,
+        out_specs=pl.BlockSpec(memory_space=pltpu.HBM),
         scratch_shapes=[pltpu.VMEM(a.shape, a.dtype) for a in sources]
-        + [pltpu.SemaphoreType.DMA((4,))],
+        + [pltpu.VMEM((slots, 2 * block + LANES), BF), pltpu.SemaphoreType.DMA((6,))],
     )
     arrived = lax.all_to_all(
         payload.reshape(n_groups, CAP, -1),
@@ -349,8 +370,9 @@
     pieces = lax.all_to_all(
         parts.reshape(widths, share, -1), "tp", split_axis=0, concat_axis=0, tiled=True
     )
-    acts = call(act_kernel, shape((share, 6 * hidden + LANES), BF), pieces, arrived)
-    acts = lax.all_gather(acts, "tp", axis=0, tiled=True)
+    acts = call(act_kernel, shape((widths, share, 6 * hidden + LANES), BF), pieces, arrived)
+    acts = lax.all_to_all(acts, "tp", split_axis=0, concat_axis=0, tiled=True)
+    acts = acts.reshape(slots, -1)
     acts = pltpu.with_memory_space_constraint(acts, pltpu.VMEM)
     back = call(
         back_kernel,

time: 130 us -> 130 us (level)
  starting transfers between devices: 47.4 us -> 50.6 us
  blocking collectives: 28.5 us -> 26.1 us
    all_gather x1 -> x0, blocking collectives: 13.6 us -> none  [body(): acts = lax.all_gather(acts, 'tp', axis=0, tiled=True)]
    all_to_all x0 -> x1, blocking collectives: none -> 12.4 us  [body(): acts = lax.all_to_all(acts, 'tp', split_axis=0, concat_axis=0, tiled=True)]
    all_to_all x1, starting transfers between devices: 11.5 us -> 14.7 us  [body(): lax.all_to_all(back.reshape(n_groups, CAP, -1), 'ep', split_axis=0, conca...]
    all_to_all x1, waiting for transfers between devices: 5.9 us -> 4.57 us  [body(): lax.all_to_all(payload.reshape(n_groups, CAP, -1), 'ep', split_axis=0, co...]
where the time goes in v4:
time: 130 us; the launch traced here: 129 us
  starting transfers between devices  50.6 us (39%)
  waiting for transfers between devices  39 us (30%)
  blocking collectives  26.1 us (20%)
  Pallas kernels  11.9 us (9%)
    all_to_all x1, starting transfers between devices, body(): lax.all_to_all(payload.reshape(n_groups, CAP, -1), 'ep', split_axis=0, co...  18.1 us
    ppermute x1, waiting for transfers between devices, body(): other = lax.ppermute(own, 'ep', partner(peers, 2))  16.8 us
    ppermute x2, waiting for transfers between devices, body(): pairs.append(lax.ppermute(pair, 'ep', partner(peers, 2)))  15.3 us
    all_to_all x1, starting transfers between devices, body(): lax.all_to_all(back.reshape(n_groups, CAP, -1), 'ep', split_axis=0, conca...  14.7 us
    all_to_all x1, blocking collectives, body(): lax.all_to_all(parts.reshape(widths, share, -1), 'tp', split_axis=0, conc...  13.8 us
    all_to_all x1, blocking collectives, body(): acts = lax.all_to_all(acts, 'tp', split_axis=0, concat_axis=0, tiled=True)  12.4 us
    pallas_call x13, Pallas kernels, call(): pl.pallas_call(kernel, out_shape=outs, compiler_params=pltpu.CompilerPara...  11.9 us
    ppermute x3, starting transfers between devices, body(): got = lax.ppermute(send, 'ep', partner(peers, 1))  6.25 us
  transfers between devices with their start and end apart: 10, of which 4 were waited for; matrix products, arithmetic and copies ran while one was open for 0% of the time, Pallas kernels for 3%

profile of v4, /device:TPU:6, one launch (start us, length us, event | category | flops | bytes accessed | tf_op | source)
XLA Modules:
  0.0 128.6 jit_solution(6627033488593003046)
XLA Ops:
  0.6 2.2 %shard_map.110 = bf16[256,1152]{1,0:T(8,128)(2,1)} custom-call(bf16[128,512]{1,0:T(8,128)(2,1)} %tok_hbm.1, bf16[128,512]{1,0:T(8,128)(2,1)} %cot_hbm.1, s32[2,128]{1,0:T(2,128)} %bitcast.29, f32[2,128]{1,0:T(2,128)} %bitcast.35), custom_call_target="tpu_custom_call" | custom-call | tf_op jit(solution)/shard_map/pallas_call | solution.py:46
  2.8 0.0 copy-start.4
  2.8 0.0 copy-start.5
  2.9 18.1 %all-to-all-start = ((bf16[32,8,1152]{2,1,0:T(8,128)(2,1)}), bf16[32,8,1152]{2,1,0:T(8,128)(2,1)S(1)}, u32[]{:S(2)}, u32[]{:S(2)}) async-start(bf16[32,8,1152]{2,1,0:T(8,128)(2,1)} %bitcast.2), calls=%async_computation | async-start | bytes 1179648 | tf_op jit(solution)/shard_map/all_to_all | solution.py:341
  21.0 0.1 pad_maximum_fusion.own_ref
  21.0 1.9 %collective-permute-start.1 = (bf16[1536,256]{1,0:T(8,128)(2,1)S(1)}, bf16[1536,256]{1,0:T(8,128)(2,1)S(1)}, u32[]{:S(2)}, u32[]{:S(2)}) collective-permute-start(bf16[1536,256]{1,0:T(8,128)(2,1)S(1)} %pad_maximum_fusion.own_ref), channel_id=1, source_target_pairs={{0,8},{4,12},{8,0},{12,4},{16,24},{20,28},{24,16},{28,20},{32,40},... | collective-permute-start | bytes 2359304 | tf_op jit(solution)/shard_map/ppermute | solution.py:351
  23.0 1.9 %collective-permute-start = (bf16[1536,256]{1,0:T(8,128)(2,1)S(1)}, bf16[1536,256]{1,0:T(8,128)(2,1)S(1)}, u32[]{:S(2)}, u32[]{:S(2)}) collective-permute-start(bf16[1536,256]{1,0:T(8,128)(2,1)S(1)} %pad_maximum_fusion.own_ref), channel_id=1, source_target_pairs={{0,4},{4,0},{8,12},{12,8},{16,20},{20,16},{24,28},{28,24},{32,36},... | collective-permute-start | bytes 2359304 | tf_op jit(solution)/shard_map/ppermute | solution.py:352
  24.9 16.8 %collective-permute-done.1.x_ref = bf16[1536,256]{1,0:T(8,128)(2,1)S(1)} collective-permute-done((bf16[1536,256]{1,0:T(8,128)(2,1)S(1)}, bf16[1536,256]{1,0:T(8,128)(2,1)S(1)}, u32[]{:S(2)}, u32[]{:S(2)}) %collective-permute-start.1) | collective-permute-done | bytes 786464 | tf_op jit(solution)/shard_map/ppermute | solution.py:351
  41.7 1.9 %collective-permute-start.2 = (bf16[1536,256]{1,0:T(8,128)(2,1)S(1)}, bf16[1536,256]{1,0:T(8,128)(2,1)}, u32[]{:S(2)}, u32[]{:S(2)}) collective-permute-start(bf16[1536,256]{1,0:T(8,128)(2,1)S(1)} %collective-permute-done.1.x_ref), channel_id=1, source_target_pairs={{0,4},{4,0},{8,12},{12,8},{16,20},{20,16},{24,28},{28,24},{32,36},... | collective-permute-start | bytes 2359304 | tf_op jit(solution)/shard_map/ppermute | solution.py:353
  43.6 2.4 %collective-permute-done.2.xsib_hbm = bf16[1536,256]{1,0:T(8,128)(2,1)} collective-permute-done((bf16[1536,256]{1,0:T(8,128)(2,1)S(1)}, bf16[1536,256]{1,0:T(8,128)(2,1)}, u32[]{:S(2)}, u32[]{:S(2)}) %collective-permute-start.2) | collective-permute-done | bytes 786464 | tf_op jit(solution)/shard_map/ppermute | solution.py:353
  46.0 4.6 %all-to-all-done = bf16[32,8,1152]{2,1,0:T(8,128)(2,1)S(1)} async-done(((bf16[32,8,1152]{2,1,0:T(8,128)(2,1)}), bf16[32,8,1152]{2,1,0:T(8,128)(2,1)S(1)}, u32[]{:S(2)}, u32[]{:S(2)}) %all-to-all-start) | async-done | bytes 589856 | tf_op jit(solution)/shard_map/all_to_all | solution.py:341
  50.5 1.6 %shard_map.111 = bf16[256,1536]{1,0:T(8,128)(2,1)S(1)} custom-call(bf16[256,1152]{1,0:T(8,128)(2,1)S(1)} %bitcast.15, bf16[1536,256]{1,0:T(8,128)(2,1)S(1)} %pad_maximum_fusion.own_ref, bf16[1536,256]{1,0:T(8,128)(2,1)S(1)} %collective-permute-done.sib_ref, bf16[1536,256]{1,0:T(8,128)(2,1)S(1)} %collective-permute-done.1.x_ref, ...), custom_call_target="tpu_custom_call" | custom-call | tf_op jit(solution)/shard_map/pallas_call | solution.py:46
  52.2 13.8 %all_to_all.20.part_ref = bf16[4,64,1536]{2,1,0:T(8,128)(2,1)S(1)} all-to-all(bf16[4,64,1536]{2,1,0:T(8,128)(2,1)S(1)} %bitcast.27), channel_id=1, replica_groups=mesh['ep'=128,'tp'=4] {'tp'}, dimensions={0} | all-to-all | bytes 1572864 | tf_op jit(solution)/shard_map/all_to_all | solution.py:370
  65.9 0.3 shard_map.112
  66.3 12.4 %all_to_all.21 = bf16[4,64,1664]{2,1,0:T(8,128)(2,1)S(1)} all-to-all(bf16[4,64,1664]{2,1,0:T(8,128)(2,1)S(1)} %shard_map.112), channel_id=1, replica_groups=mesh['ep'=128,'tp'=4] {'tp'}, dimensions={0} | all-to-all | bytes 1703936 | tf_op jit(solution)/shard_map/all_to_all | solution.py:374
  78.6 2.2 %shard_map.113 = bf16[256,640]{1,0:T(8,128)(2,1)} custom-call(bf16[256,1664]{1,0:T(8,128)(2,1)S(1)} %bitcast.22, bf16[256,1152]{1,0:T(8,128)(2,1)S(1)} %bitcast.17, bf16[1536,256]{1,0:T(8,128)(2,1)S(1)} %pad_maximum_fusion.own_ref, bf16[1536,256]{1,0:T(8,128)(2,1)S(1)} %copy-done.1, bf16[1536,256]{1,0:T(8,128)(2,1)S(1)} %collective-permute-done.1.x_ref, ...), custom_call_target="tpu_custom_call" | custom-call | tf_op jit(solution)/shard_map/pallas_call | solution.py:46
  80.9 14.7 %all-to-all-start.3 = ((bf16[32,8,640]{2,1,0:T(8,128)(2,1)}), bf16[32,8,640]{2,1,0:T(8,128)(2,1)S(1)}, u32[]{:S(2)}, u32[]{:S(2)}) async-start(bf16[32,8,640]{2,1,0:T(8,128)(2,1)} %bitcast.9), calls=%async_computation.3 | async-start | bytes 655360 | tf_op jit(solution)/shard_map/all_to_all | solution.py:386
  95.6 0.7 shard_map.117
  96.3 1.9 %collective-permute-start.4 = (bf16[1024,256]{1,0:T(8,128)(2,1)S(1)}, bf16[1024,256]{1,0:T(8,128)(2,1)S(1)}, u32[]{:S(2)}, u32[]{:S(2)}) collective-permute-start(bf16[1024,256]{1,0:T(8,128)(2,1)S(1)} %get-tuple-element.19), channel_id=1, source_target_pairs={{0,4},{4,0},{8,12},{12,8},{16,20},{20,16},{24,28},{28,24},{32,36},... | collective-permute-start | bytes 1572872 | tf_op jit(solution)/shard_map/ppermute | solution.py:400
  98.2 0.6 shard_map.115
  98.8 2.4 %collective-permute-start.3 = (bf16[1536,256]{1,0:T(8,128)(2,1)S(1)}, bf16[1536,256]{1,0:T(8,128)(2,1)S(1)}, u32[]{:S(2)}, u32[]{:S(2)}) collective-permute-start(bf16[1536,256]{1,0:T(8,128)(2,1)S(1)} %shard_map.115), channel_id=1, source_target_pairs={{0,4},{4,0},{8,12},{12,8},{16,20},{20,16},{24,28},{28,24},{32,36},... | collective-permute-start | bytes 2359304 | tf_op jit(solution)/shard_map/ppermute | solution.py:404
  101.2 0.6 shard_map.120
  101.8 1.9 %collective-permute-start.6 = (bf16[256,512]{1,0:T(8,128)(2,1)S(1)}, bf16[256,512]{1,0:T(8,128)(2,1)S(1)}, u32[]{:S(2)}, u32[]{:S(2)}) collective-permute-start(bf16[256,512]{1,0:T(8,128)(2,1)S(1)} %get-tuple-element.24), channel_id=1, source_target_pairs={{0,4},{4,0},{8,12},{12,8},{16,20},{20,16},{24,28},{28,24},{32,36},... | collective-permute-start | bytes 786440 | tf_op jit(solution)/shard_map/ppermute | solution.py:400
  103.7 0.1 shard_map.118
  103.9 1.9 %collective-permute-start.5 = (bf16[1024,256]{1,0:T(8,128)(2,1)S(1)}, bf16[1024,256]{1,0:T(8,128)(2,1)S(1)}, u32[]{:S(2)}, u32[]{:S(2)}) collective-permute-start(bf16[1024,256]{1,0:T(8,128)(2,1)S(1)} %shard_map.118), channel_id=1, source_target_pairs={{0,8},{4,12},{8,0},{12,4},{16,24},{20,28},{24,16},{28,20},{32,40},... | collective-permute-start | bytes 1572872 | tf_op jit(solution)/shard_map/ppermute | solution.py:402
  105.8 0.1 shard_map.121
  105.9 3.9 %collective-permute-start.7 = (bf16[256,512]{1,0:T(8,128)(2,1)S(1)}, bf16[256,512]{1,0:T(8,128)(2,1)S(1)}, u32[]{:S(2)}, u32[]{:S(2)}) collective-permute-start(bf16[256,512]{1,0:T(8,128)(2,1)S(1)} %shard_map.121), channel_id=1, source_target_pairs={{0,8},{4,12},{8,0},{12,4},{16,24},{20,28},{24,16},{28,20},{32,40},... | collective-permute-start | bytes 786440 | tf_op jit(solution)/shard_map/ppermute | solution.py:402
  109.8 0.6 shard_map.116
  110.4 15.3 %collective-permute-done.7.last_ref = bf16[256,512]{1,0:T(8,128)(2,1)S(1)} collective-permute-done((bf16[256,512]{1,0:T(8,128)(2,1)S(1)}, bf16[256,512]{1,0:T(8,128)(2,1)S(1)}, u32[]{:S(2)}, u32[]{:S(2)}) %collective-permute-start.7) | collective-permute-done | bytes 262176 | tf_op jit(solution)/shard_map/ppermute | solution.py:402
  125.7 0.8 shard_map.122
  126.5 1.0 shard_map.119
  127.6 1.0 shard_map.114
  (17 shorter events, 0.1 us)
Async XLA Ops:
  0.6 20.3 %copy-start.3 = (bf16[1,256,512]{2,1,0:T(8,128)(2,1)S(1)}, bf16[1,256,512]{2,1,0:T(8,128)(2,1)}, u32[]{:S(2)}) copy-start(bf16[1,256,512]{2,1,0:T(8,128)(2,1)} %param.13) | copy-start | bytes 786436
  2.8 18.1 %copy-start.4 = (bf16[1,512,256]{2,1,0:T(8,128)(2,1)S(1)}, bf16[1,512,256]{2,1,0:T(8,128)(2,1)}, u32[]{:S(2)}) copy-start(bf16[1,512,256]{2,1,0:T(8,128)(2,1)} %param.12) | copy-start | bytes 786436
  2.8 18.1 %copy-start.5 = (bf16[1,512,256]{2,1,0:T(8,128)(2,1)S(1)}, bf16[1,512,256]{2,1,0:T(8,128)(2,1)}, u32[]{:S(2)}) copy-start(bf16[1,512,256]{2,1,0:T(8,128)(2,1)} %param.11) | copy-start | bytes 786436
  2.9 47.7 %all-to-all-start = ((bf16[32,8,1152]{2,1,0:T(8,128)(2,1)}), bf16[32,8,1152]{2,1,0:T(8,128)(2,1)S(1)}, u32[]{:S(2)}, u32[]{:S(2)}) async-start(bf16[32,8,1152]{2,1,0:T(8,128)(2,1)} %bitcast.2), calls=%async_computation | async-start | bytes 1179648 | tf_op jit(solution)/shard_map/all_to_all | solution.py:341
  21.0 20.6 %collective-permute-start.1 = (bf16[1536,256]{1,0:T(8,128)(2,1)S(1)}, bf16[1536,256]{1,0:T(8,128)(2,1)S(1)}, u32[]{:S(2)}, u32[]{:S(2)}) collective-permute-start(bf16[1536,256]{1,0:T(8,128)(2,1)S(1)} %pad_maximum_fusion.own_ref), channel_id=1, source_target_pairs={{0,8},{4,12},{8,0},{12,4},{16,24},{20,28},{24,16},{28,20},{32,40},... | collective-permute-start | bytes 2359304 | tf_op jit(solution)/shard_map/ppermute | solution.py:351
  23.0 20.6 %collective-permute-start = (bf16[1536,256]{1,0:T(8,128)(2,1)S(1)}, bf16[1536,256]{1,0:T(8,128)(2,1)S(1)}, u32[]{:S(2)}, u32[]{:S(2)}) collective-permute-start(bf16[1536,256]{1,0:T(8,128)(2,1)S(1)} %pad_maximum_fusion.own_ref), channel_id=1, source_target_pairs={{0,4},{4,0},{8,12},{12,8},{16,20},{20,16},{24,28},{28,24},{32,36},... | collective-permute-start | bytes 2359304 | tf_op jit(solution)/shard_map/ppermute | solution.py:352
  41.7 4.3 %collective-permute-start.2 = (bf16[1536,256]{1,0:T(8,128)(2,1)S(1)}, bf16[1536,256]{1,0:T(8,128)(2,1)}, u32[]{:S(2)}, u32[]{:S(2)}) collective-permute-start(bf16[1536,256]{1,0:T(8,128)(2,1)S(1)} %collective-permute-done.1.x_ref), channel_id=1, source_target_pairs={{0,4},{4,0},{8,12},{12,8},{16,20},{20,16},{24,28},{28,24},{32,36},... | collective-permute-start | bytes 2359304 | tf_op jit(solution)/shard_map/ppermute | solution.py:353
  43.6 8.6 %copy-start = (bf16[1536,256]{1,0:T(8,128)(2,1)}, bf16[1536,256]{1,0:T(8,128)(2,1)S(1)}, u32[]{:S(2)}) copy-start(bf16[1536,256]{1,0:T(8,128)(2,1)S(1)} %collective-permute-done.sib_ref) | copy-start | bytes 2359300
  66.3 12.4 %copy-start.1 = (bf16[1536,256]{1,0:T(8,128)(2,1)S(1)}, bf16[1536,256]{1,0:T(8,128)(2,1)}, u32[]{:S(2)}) copy-start(bf16[1536,256]{1,0:T(8,128)(2,1)} %copy-done) | copy-start | bytes 2359300
  80.9 46.7 %all-to-all-start.3 = ((bf16[32,8,640]{2,1,0:T(8,128)(2,1)}), bf16[32,8,640]{2,1,0:T(8,128)(2,1)S(1)}, u32[]{:S(2)}, u32[]{:S(2)}) async-start(bf16[32,8,640]{2,1,0:T(8,128)(2,1)} %bitcast.9), calls=%async_computation.3 | async-start | bytes 655360 | tf_op jit(solution)/shard_map/all_to_all | solution.py:386
  96.3 7.4 %collective-permute-start.4 = (bf16[1024,256]{1,0:T(8,128)(2,1)S(1)}, bf16[1024,256]{1,0:T(8,128)(2,1)S(1)}, u32[]{:S(2)}, u32[]{:S(2)}) collective-permute-start(bf16[1024,256]{1,0:T(8,128)(2,1)S(1)} %get-tuple-element.19), channel_id=1, source_target_pairs={{0,4},{4,0},{8,12},{12,8},{16,20},{20,16},{24,28},{28,24},{32,36},... | collective-permute-start | bytes 1572872 | tf_op jit(solution)/shard_map/ppermute | solution.py:400
  98.8 11.0 %collective-permute-start.3 = (bf16[1536,256]{1,0:T(8,128)(2,1)S(1)}, bf16[1536,256]{1,0:T(8,128)(2,1)S(1)}, u32[]{:S(2)}, u32[]{:S(2)}) collective-permute-start(bf16[1536,256]{1,0:T(8,128)(2,1)S(1)} %shard_map.115), channel_id=1, source_target_pairs={{0,4},{4,0},{8,12},{12,8},{16,20},{20,16},{24,28},{28,24},{32,36},... | collective-permute-start | bytes 2359304 | tf_op jit(solution)/shard_map/ppermute | solution.py:404
  101.8 4.0 %collective-permute-start.6 = (bf16[256,512]{1,0:T(8,128)(2,1)S(1)}, bf16[256,512]{1,0:T(8,128)(2,1)S(1)}, u32[]{:S(2)}, u32[]{:S(2)}) collective-permute-start(bf16[256,512]{1,0:T(8,128)(2,1)S(1)} %get-tuple-element.24), channel_id=1, source_target_pairs={{0,4},{4,0},{8,12},{12,8},{16,20},{20,16},{24,28},{28,24},{32,36},... | collective-permute-start | bytes 786440 | tf_op jit(solution)/shard_map/ppermute | solution.py:400
  103.9 22.7 %collective-permute-start.5 = (bf16[1024,256]{1,0:T(8,128)(2,1)S(1)}, bf16[1024,256]{1,0:T(8,128)(2,1)S(1)}, u32[]{:S(2)}, u32[]{:S(2)}) collective-permute-start(bf16[1024,256]{1,0:T(8,128)(2,1)S(1)} %shard_map.118), channel_id=1, source_target_pairs={{0,8},{4,12},{8,0},{12,4},{16,24},{20,28},{24,16},{28,20},{32,40},... | collective-permute-start | bytes 1572872 | tf_op jit(solution)/shard_map/ppermute | solution.py:402
  105.9 19.8 %collective-permute-start.7 = (bf16[256,512]{1,0:T(8,128)(2,1)S(1)}, bf16[256,512]{1,0:T(8,128)(2,1)S(1)}, u32[]{:S(2)}, u32[]{:S(2)}) collective-permute-start(bf16[256,512]{1,0:T(8,128)(2,1)S(1)} %shard_map.121), channel_id=1, source_target_pairs={{0,8},{4,12},{8,0},{12,4},{16,24},{20,28},{24,16},{28,20},{32,40},... | collective-permute-start | bytes 786440 | tf_op jit(solution)/shard_map/ppermute | solution.py:402
  125.7 1.9 %copy-start.2 = (s32[128,2]{0,1:T(2,128)S(1)}, s32[128,2]{0,1:T(2,128)}, u32[]{:S(2)}) copy-start(s32[128,2]{0,1:T(2,128)} %param.9) | copy-start | bytes 3076

commit v5 on v4

--- a/solution.py
+++ b/solution.py
@@ -169,11 +169,6 @@
     hidden = part_ref.shape[2] // 6
     meta_at = arr_ref.shape[1] - LANES
     me = lax.axis_index("tp")
-
-    def put(at, value):
-        for copy in range(out_ref.shape[0]):
-            out_ref[copy, :, at : at + value.shape[1]] = value
-
     meta = arr_ref[pl.ds(pl.multiple_of(me * share, share), share), meta_at:].astype(F32)
     first, second = chosen(meta)
     lane = iota((share, LANES), 1)
@@ -193,13 +188,15 @@
         hid = silu * up_pre
         gh = weight * grad_scaled
         at = 3 * k * hidden
-        put(at, (weight * hid).astype(BF))
-        put(at + hidden, (gh * up_pre * sig * (1.0 + gate_pre * (1.0 - sig))).astype(BF))
-        put(at + 2 * hidden, (gh * silu).astype(BF))
+        out_ref[:, at : at + hidden] = (weight * hid).astype(BF)
+        out_ref[:, at + hidden : at + 2 * hidden] = (
+            gh * up_pre * sig * (1.0 + gate_pre * (1.0 - sig))
+        ).astype(BF)
+        out_ref[:, at + 2 * hidden : at + 3 * hidden] = (gh * silu).astype(BF)
         comb = jnp.sum(hid * grad_scaled, axis=1, keepdims=True)
         high = comb.astype(BF).astype(F32)
         extra = jnp.where(lane == 2 * k, high, jnp.where(lane == 2 * k + 1, comb - high, extra))
-    put(6 * hidden, extra.astype(BF))
+    out_ref[:, 6 * hidden :] = extra.astype(BF)
 
 
 def masks(arr_ref, hidden, experts=ORDER):
@@ -370,9 +367,8 @@
     pieces = lax.all_to_all(
         parts.reshape(widths, share, -1), "tp", split_axis=0, concat_axis=0, tiled=True
     )
-    acts = call(act_kernel, shape((widths, share, 6 * hidden + LANES), BF), pieces, arrived)
-    acts = lax.all_to_all(acts, "tp", split_axis=0, concat_axis=0, tiled=True)
-    acts = acts.reshape(slots, -1)
+    acts = call(act_kernel, shape((share, 6 * hidden + LANES), BF), pieces, arrived)
+    acts = lax.all_gather(acts, "tp", axis=0, tiled=True)
     acts = pltpu.with_memory_space_constraint(acts, pltpu.VMEM)
     back = call(
         back_kernel,

time: 130 us -> 130 us (level)
  starting transfers between devices: 50.6 us -> 48.4 us
  blocking collectives: 26.1 us -> 28.2 us
    all_gather x0 -> x1, blocking collectives: none -> 13.7 us  [body(): acts = lax.all_gather(acts, 'tp', axis=0, tiled=True)]
    all_to_all x1 -> x0, blocking collectives: 12.4 us -> none  [body(): acts = lax.all_to_all(acts, 'tp', split_axis=0, concat_axis=0, tiled=True)]
    all_to_all x1, starting transfers between devices: 14.7 us -> 12.5 us  [body(): lax.all_to_all(back.reshape(n_groups, CAP, -1), 'ep', split_axis=0, conca...]
where the time goes in v5:
time: 130 us; the launch traced here: 128 us
  starting transfers between devices  48.4 us (37%)
  waiting for transfers between devices  39 us (30%)
  blocking collectives  28.2 us (22%)
  Pallas kernels  11.8 us (9%)
    all_to_all x1, starting transfers between devices, body(): lax.all_to_all(payload.reshape(n_groups, CAP, -1), 'ep', split_axis=0, co...  18.1 us
    ppermute x1, waiting for transfers between devices, body(): other = lax.ppermute(own, 'ep', partner(peers, 2))  16.8 us
    ppermute x2, waiting for transfers between devices, body(): pairs.append(lax.ppermute(pair, 'ep', partner(peers, 2)))  15.3 us
    all_to_all x1, blocking collectives, body(): lax.all_to_all(parts.reshape(widths, share, -1), 'tp', split_axis=0, conc...  14.5 us
    all_gather x1, blocking collectives, body(): acts = lax.all_gather(acts, 'tp', axis=0, tiled=True)  13.7 us
    all_to_all x1, starting transfers between devices, body(): lax.all_to_all(back.reshape(n_groups, CAP, -1), 'ep', split_axis=0, conca...  12.5 us
    pallas_call x13, Pallas kernels, call(): pl.pallas_call(kernel, out_shape=outs, compiler_params=pltpu.CompilerPara...  11.8 us
    ppermute x3, starting transfers between devices, body(): got = lax.ppermute(send, 'ep', partner(peers, 1))  6.25 us
  transfers between devices with their start and end apart: 10, of which 4 were waited for; matrix products, arithmetic and copies ran while one was open for 0% of the time, Pallas kernels for 3%

profile of v5, /device:TPU:6, one launch (start us, length us, event | category | flops | bytes accessed | tf_op | source)
XLA Modules:
  0.0 128.5 jit_solution(4265641637295335553)
XLA Ops:
  0.6 2.2 %shard_map.110 = bf16[256,1152]{1,0:T(8,128)(2,1)} custom-call(bf16[128,512]{1,0:T(8,128)(2,1)} %tok_hbm.1, bf16[128,512]{1,0:T(8,128)(2,1)} %cot_hbm.1, s32[2,128]{1,0:T(2,128)} %bitcast.23, f32[2,128]{1,0:T(2,128)} %bitcast.29), custom_call_target="tpu_custom_call" | custom-call | tf_op jit(solution)/shard_map/pallas_call | solution.py:46
  2.8 0.0 copy-start.4
  2.8 0.0 copy-start.5
  2.9 18.1 %all-to-all-start = ((bf16[32,8,1152]{2,1,0:T(8,128)(2,1)}), bf16[32,8,1152]{2,1,0:T(8,128)(2,1)S(1)}, u32[]{:S(2)}, u32[]{:S(2)}) async-start(bf16[32,8,1152]{2,1,0:T(8,128)(2,1)} %bitcast.2), calls=%async_computation | async-start | bytes 1179648 | tf_op jit(solution)/shard_map/all_to_all | solution.py:338
  21.0 0.1 pad_maximum_fusion.own_ref
  21.0 1.9 %collective-permute-start.1 = (bf16[1536,256]{1,0:T(8,128)(2,1)S(1)}, bf16[1536,256]{1,0:T(8,128)(2,1)S(1)}, u32[]{:S(2)}, u32[]{:S(2)}) collective-permute-start(bf16[1536,256]{1,0:T(8,128)(2,1)S(1)} %pad_maximum_fusion.own_ref), channel_id=1, source_target_pairs={{0,8},{4,12},{8,0},{12,4},{16,24},{20,28},{24,16},{28,20},{32,40},... | collective-permute-start | bytes 2359304 | tf_op jit(solution)/shard_map/ppermute | solution.py:348
  23.0 1.9 %collective-permute-start = (bf16[1536,256]{1,0:T(8,128)(2,1)S(1)}, bf16[1536,256]{1,0:T(8,128)(2,1)S(1)}, u32[]{:S(2)}, u32[]{:S(2)}) collective-permute-start(bf16[1536,256]{1,0:T(8,128)(2,1)S(1)} %pad_maximum_fusion.own_ref), channel_id=1, source_target_pairs={{0,4},{4,0},{8,12},{12,8},{16,20},{20,16},{24,28},{28,24},{32,36},... | collective-permute-start | bytes 2359304 | tf_op jit(solution)/shard_map/ppermute | solution.py:349
  24.9 16.8 %collective-permute-done.1.x_ref = bf16[1536,256]{1,0:T(8,128)(2,1)S(1)} collective-permute-done((bf16[1536,256]{1,0:T(8,128)(2,1)S(1)}, bf16[1536,256]{1,0:T(8,128)(2,1)S(1)}, u32[]{:S(2)}, u32[]{:S(2)}) %collective-permute-start.1) | collective-permute-done | bytes 786464 | tf_op jit(solution)/shard_map/ppermute | solution.py:348
  41.7 1.9 %collective-permute-start.2 = (bf16[1536,256]{1,0:T(8,128)(2,1)S(1)}, bf16[1536,256]{1,0:T(8,128)(2,1)}, u32[]{:S(2)}, u32[]{:S(2)}) collective-permute-start(bf16[1536,256]{1,0:T(8,128)(2,1)S(1)} %collective-permute-done.1.x_ref), channel_id=1, source_target_pairs={{0,4},{4,0},{8,12},{12,8},{16,20},{20,16},{24,28},{28,24},{32,36},... | collective-permute-start | bytes 2359304 | tf_op jit(solution)/shard_map/ppermute | solution.py:350
  43.6 2.4 %collective-permute-done.2.xsib_hbm = bf16[1536,256]{1,0:T(8,128)(2,1)} collective-permute-done((bf16[1536,256]{1,0:T(8,128)(2,1)S(1)}, bf16[1536,256]{1,0:T(8,128)(2,1)}, u32[]{:S(2)}, u32[]{:S(2)}) %collective-permute-start.2) | collective-permute-done | bytes 786464 | tf_op jit(solution)/shard_map/ppermute | solution.py:350
  46.0 4.6 %all-to-all-done = bf16[32,8,1152]{2,1,0:T(8,128)(2,1)S(1)} async-done(((bf16[32,8,1152]{2,1,0:T(8,128)(2,1)}), bf16[32,8,1152]{2,1,0:T(8,128)(2,1)S(1)}, u32[]{:S(2)}, u32[]{:S(2)}) %all-to-all-start) | async-done | bytes 589856 | tf_op jit(solution)/shard_map/all_to_all | solution.py:338
  50.5 1.6 %shard_map.111 = bf16[256,1536]{1,0:T(8,128)(2,1)S(1)} custom-call(bf16[256,1152]{1,0:T(8,128)(2,1)S(1)} %bitcast.14, bf16[1536,256]{1,0:T(8,128)(2,1)S(1)} %pad_maximum_fusion.own_ref, bf16[1536,256]{1,0:T(8,128)(2,1)S(1)} %collective-permute-done.sib_ref, bf16[1536,256]{1,0:T(8,128)(2,1)S(1)} %collective-permute-done.1.x_ref, ...), custom_call_target="tpu_custom_call" | custom-call | tf_op jit(solution)/shard_map/pallas_call | solution.py:46
  52.2 14.5 %all_to_all.15.part_ref = bf16[4,64,1536]{2,1,0:T(8,128)(2,1)S(1)} all-to-all(bf16[4,64,1536]{2,1,0:T(8,128)(2,1)S(1)} %bitcast.21), channel_id=1, replica_groups=mesh['ep'=128,'tp'=4] {'tp'}, dimensions={0} | all-to-all | bytes 1572864 | tf_op jit(solution)/shard_map/all_to_all | solution.py:367
  66.7 0.3 shard_map.112
  67.0 13.7 %all_gather.3.act_ref = bf16[256,1664]{1,0:T(8,128)(2,1)S(1)} all-gather(bf16[64,1664]{1,0:T(8,128)(2,1)S(1)} %shard_map.112), channel_id=1, replica_groups=mesh['ep'=128,'tp'=4] {'tp'}, dimensions={0}, use_global_device_ids=true | all-gather | bytes 1064960 | tf_op jit(solution)/shard_map/all_gather | solution.py:371
  80.7 2.2 %shard_map.113 = bf16[256,640]{1,0:T(8,128)(2,1)} custom-call(bf16[256,1664]{1,0:T(8,128)(2,1)S(1)} %all_gather.3.act_ref, bf16[256,1152]{1,0:T(8,128)(2,1)S(1)} %bitcast.16, bf16[1536,256]{1,0:T(8,128)(2,1)S(1)} %pad_maximum_fusion.own_ref, bf16[1536,256]{1,0:T(8,128)(2,1)S(1)} %copy-done.1, bf16[1536,256]{1,0:T(8,128)(2,1)S(1)} %collective-permute-done.1.x_ref, ...), custom_call_target="tpu_custom_call" | custom-call | tf_op jit(solution)/shard_map/pallas_call | solution.py:46
  83.0 12.5 %all-to-all-start.2 = ((bf16[32,8,640]{2,1,0:T(8,128)(2,1)}), bf16[32,8,640]{2,1,0:T(8,128)(2,1)S(1)}, u32[]{:S(2)}, u32[]{:S(2)}) async-start(bf16[32,8,640]{2,1,0:T(8,128)(2,1)} %bitcast.8), calls=%async_computation.2 | async-start | bytes 655360 | tf_op jit(solution)/shard_map/all_to_all | solution.py:382
  95.5 0.7 shard_map.117
  96.2 1.9 %collective-permute-start.4 = (bf16[1024,256]{1,0:T(8,128)(2,1)S(1)}, bf16[1024,256]{1,0:T(8,128)(2,1)S(1)}, u32[]{:S(2)}, u32[]{:S(2)}) collective-permute-start(bf16[1024,256]{1,0:T(8,128)(2,1)S(1)} %get-tuple-element.19), channel_id=1, source_target_pairs={{0,4},{4,0},{8,12},{12,8},{16,20},{20,16},{24,28},{28,24},{32,36},... | collective-permute-start | bytes 1572872 | tf_op jit(solution)/shard_map/ppermute | solution.py:396
  98.1 0.6 shard_map.115
  98.7 2.4 %collective-permute-start.3 = (bf16[1536,256]{1,0:T(8,128)(2,1)S(1)}, bf16[1536,256]{1,0:T(8,128)(2,1)S(1)}, u32[]{:S(2)}, u32[]{:S(2)}) collective-permute-start(bf16[1536,256]{1,0:T(8,128)(2,1)S(1)} %shard_map.115), channel_id=1, source_target_pairs={{0,4},{4,0},{8,12},{12,8},{16,20},{20,16},{24,28},{28,24},{32,36},... | collective-permute-start | bytes 2359304 | tf_op jit(solution)/shard_map/ppermute | solution.py:400
  101.1 0.6 shard_map.120
  101.7 1.9 %collective-permute-start.6 = (bf16[256,512]{1,0:T(8,128)(2,1)S(1)}, bf16[256,512]{1,0:T(8,128)(2,1)S(1)}, u32[]{:S(2)}, u32[]{:S(2)}) collective-permute-start(bf16[256,512]{1,0:T(8,128)(2,1)S(1)} %get-tuple-element.24), channel_id=1, source_target_pairs={{0,4},{4,0},{8,12},{12,8},{16,20},{20,16},{24,28},{28,24},{32,36},... | collective-permute-start | bytes 786440 | tf_op jit(solution)/shard_map/ppermute | solution.py:396
  103.6 0.1 shard_map.118
  103.7 1.9 %collective-permute-start.5 = (bf16[1024,256]{1,0:T(8,128)(2,1)S(1)}, bf16[1024,256]{1,0:T(8,128)(2,1)S(1)}, u32[]{:S(2)}, u32[]{:S(2)}) collective-permute-start(bf16[1024,256]{1,0:T(8,128)(2,1)S(1)} %shard_map.118), channel_id=1, source_target_pairs={{0,8},{4,12},{8,0},{12,4},{16,24},{20,28},{24,16},{28,20},{32,40},... | collective-permute-start | bytes 1572872 | tf_op jit(solution)/shard_map/ppermute | solution.py:398
  105.7 0.1 shard_map.121
  105.8 3.9 %collective-permute-start.7 = (bf16[256,512]{1,0:T(8,128)(2,1)S(1)}, bf16[256,512]{1,0:T(8,128)(2,1)S(1)}, u32[]{:S(2)}, u32[]{:S(2)}) collective-permute-start(bf16[256,512]{1,0:T(8,128)(2,1)S(1)} %shard_map.121), channel_id=1, source_target_pairs={{0,8},{4,12},{8,0},{12,4},{16,24},{20,28},{24,16},{28,20},{32,40},... | collective-permute-start | bytes 786440 | tf_op jit(solution)/shard_map/ppermute | solution.py:398
  109.7 0.6 shard_map.116
  110.3 15.3 %collective-permute-done.7.last_ref = bf16[256,512]{1,0:T(8,128)(2,1)S(1)} collective-permute-done((bf16[256,512]{1,0:T(8,128)(2,1)S(1)}, bf16[256,512]{1,0:T(8,128)(2,1)S(1)}, u32[]{:S(2)}, u32[]{:S(2)}) %collective-permute-start.7) | collective-permute-done | bytes 262176 | tf_op jit(solution)/shard_map/ppermute | solution.py:398
  125.6 0.8 shard_map.122
  126.4 1.0 shard_map.119
  127.4 1.0 shard_map.114
  (17 shorter events, 0.1 us)
Async XLA Ops:
  0.6 20.3 %copy-start.3 = (bf16[1,256,512]{2,1,0:T(8,128)(2,1)S(1)}, bf16[1,256,512]{2,1,0:T(8,128)(2,1)}, u32[]{:S(2)}) copy-start(bf16[1,256,512]{2,1,0:T(8,128)(2,1)} %param.13) | copy-start | bytes 786436
  2.8 18.1 %copy-start.4 = (bf16[1,512,256]{2,1,0:T(8,128)(2,1)S(1)}, bf16[1,512,256]{2,1,0:T(8,128)(2,1)}, u32[]{:S(2)}) copy-start(bf16[1,512,256]{2,1,0:T(8,128)(2,1)} %param.12) | copy-start | bytes 786436
  2.8 18.1 %copy-start.5 = (bf16[1,512,256]{2,1,0:T(8,128)(2,1)S(1)}, bf16[1,512,256]{2,1,0:T(8,128)(2,1)}, u32[]{:S(2)}) copy-start(bf16[1,512,256]{2,1,0:T(8,128)(2,1)} %param.11) | copy-start | bytes 786436
  2.9 47.7 %all-to-all-start = ((bf16[32,8,1152]{2,1,0:T(8,128)(2,1)}), bf16[32,8,1152]{2,1,0:T(8,128)(2,1)S(1)}, u32[]{:S(2)}, u32[]{:S(2)}) async-start(bf16[32,8,1152]{2,1,0:T(8,128)(2,1)} %bitcast.2), calls=%async_computation | async-start | bytes 1179648 | tf_op jit(solution)/shard_map/all_to_all | solution.py:338
  21.0 20.6 %collective-permute-start.1 = (bf16[1536,256]{1,0:T(8,128)(2,1)S(1)}, bf16[1536,256]{1,0:T(8,128)(2,1)S(1)}, u32[]{:S(2)}, u32[]{:S(2)}) collective-permute-start(bf16[1536,256]{1,0:T(8,128)(2,1)S(1)} %pad_maximum_fusion.own_ref), channel_id=1, source_target_pairs={{0,8},{4,12},{8,0},{12,4},{16,24},{20,28},{24,16},{28,20},{32,40},... | collective-permute-start | bytes 2359304 | tf_op jit(solution)/shard_map/ppermute | solution.py:348
  23.0 20.6 %collective-permute-start = (bf16[1536,256]{1,0:T(8,128)(2,1)S(1)}, bf16[1536,256]{1,0:T(8,128)(2,1)S(1)}, u32[]{:S(2)}, u32[]{:S(2)}) collective-permute-start(bf16[1536,256]{1,0:T(8,128)(2,1)S(1)} %pad_maximum_fusion.own_ref), channel_id=1, source_target_pairs={{0,4},{4,0},{8,12},{12,8},{16,20},{20,16},{24,28},{28,24},{32,36},... | collective-permute-start | bytes 2359304 | tf_op jit(solution)/shard_map/ppermute | solution.py:349
  41.7 4.3 %collective-permute-start.2 = (bf16[1536,256]{1,0:T(8,128)(2,1)S(1)}, bf16[1536,256]{1,0:T(8,128)(2,1)}, u32[]{:S(2)}, u32[]{:S(2)}) collective-permute-start(bf16[1536,256]{1,0:T(8,128)(2,1)S(1)} %collective-permute-done.1.x_ref), channel_id=1, source_target_pairs={{0,4},{4,0},{8,12},{12,8},{16,20},{20,16},{24,28},{28,24},{32,36},... | collective-permute-start | bytes 2359304 | tf_op jit(solution)/shard_map/ppermute | solution.py:350
  43.6 8.6 %copy-start = (bf16[1536,256]{1,0:T(8,128)(2,1)}, bf16[1536,256]{1,0:T(8,128)(2,1)S(1)}, u32[]{:S(2)}) copy-start(bf16[1536,256]{1,0:T(8,128)(2,1)S(1)} %collective-permute-done.sib_ref) | copy-start | bytes 2359300
  67.0 13.8 %copy-start.1 = (bf16[1536,256]{1,0:T(8,128)(2,1)S(1)}, bf16[1536,256]{1,0:T(8,128)(2,1)}, u32[]{:S(2)}) copy-start(bf16[1536,256]{1,0:T(8,128)(2,1)} %copy-done) | copy-start | bytes 2359300
  83.0 44.5 %all-to-all-start.2 = ((bf16[32,8,640]{2,1,0:T(8,128)(2,1)}), bf16[32,8,640]{2,1,0:T(8,128)(2,1)S(1)}, u32[]{:S(2)}, u32[]{:S(2)}) async-start(bf16[32,8,640]{2,1,0:T(8,128)(2,1)} %bitcast.8), calls=%async_computation.2 | async-start | bytes 655360 | tf_op jit(solution)/shard_map/all_to_all | solution.py:382
  96.2 7.4 %collective-permute-start.4 = (bf16[1024,256]{1,0:T(8,128)(2,1)S(1)}, bf16[1024,256]{1,0:T(8,128)(2,1)S(1)}, u32[]{:S(2)}, u32[]{:S(2)}) collective-permute-start(bf16[1024,256]{1,0:T(8,128)(2,1)S(1)} %get-tuple-element.19), channel_id=1, source_target_pairs={{0,4},{4,0},{8,12},{12,8},{16,20},{20,16},{24,28},{28,24},{32,36},... | collective-permute-start | bytes 1572872 | tf_op jit(solution)/shard_map/ppermute | solution.py:396
  98.7 11.0 %collective-permute-start.3 = (bf16[1536,256]{1,0:T(8,128)(2,1)S(1)}, bf16[1536,256]{1,0:T(8,128)(2,1)S(1)}, u32[]{:S(2)}, u32[]{:S(2)}) collective-permute-start(bf16[1536,256]{1,0:T(8,128)(2,1)S(1)} %shard_map.115), channel_id=1, source_target_pairs={{0,4},{4,0},{8,12},{12,8},{16,20},{20,16},{24,28},{28,24},{32,36},... | collective-permute-start | bytes 2359304 | tf_op jit(solution)/shard_map/ppermute | solution.py:400
  101.7 4.0 %collective-permute-start.6 = (bf16[256,512]{1,0:T(8,128)(2,1)S(1)}, bf16[256,512]{1,0:T(8,128)(2,1)S(1)}, u32[]{:S(2)}, u32[]{:S(2)}) collective-permute-start(bf16[256,512]{1,0:T(8,128)(2,1)S(1)} %get-tuple-element.24), channel_id=1, source_target_pairs={{0,4},{4,0},{8,12},{12,8},{16,20},{20,16},{24,28},{28,24},{32,36},... | collective-permute-start | bytes 786440 | tf_op jit(solution)/shard_map/ppermute | solution.py:396
  103.7 22.7 %collective-permute-start.5 = (bf16[1024,256]{1,0:T(8,128)(2,1)S(1)}, bf16[1024,256]{1,0:T(8,128)(2,1)S(1)}, u32[]{:S(2)}, u32[]{:S(2)}) collective-permute-start(bf16[1024,256]{1,0:T(8,128)(2,1)S(1)} %shard_map.118), channel_id=1, source_target_pairs={{0,8},{4,12},{8,0},{12,4},{16,24},{20,28},{24,16},{28,20},{32,40},... | collective-permute-start | bytes 1572872 | tf_op jit(solution)/shard_map/ppermute | solution.py:398
  105.8 19.8 %collective-permute-start.7 = (bf16[256,512]{1,0:T(8,128)(2,1)S(1)}, bf16[256,512]{1,0:T(8,128)(2,1)S(1)}, u32[]{:S(2)}, u32[]{:S(2)}) collective-permute-start(bf16[256,512]{1,0:T(8,128)(2,1)S(1)} %shard_map.121), channel_id=1, source_target_pairs={{0,8},{4,12},{8,0},{12,4},{16,24},{20,28},{24,16},{28,20},{32,40},... | collective-permute-start | bytes 786440 | tf_op jit(solution)/shard_map/ppermute | solution.py:398
  125.6 1.9 %copy-start.2 = (s32[128,2]{0,1:T(2,128)S(1)}, s32[128,2]{0,1:T(2,128)}, u32[]{:S(2)}) copy-start(s32[128,2]{0,1:T(2,128)} %param.9) | copy-start | bytes 3076
